TPU v7x, 32 devices: a whole 2x2x4 slice. The times are simulated.
32 devices in a mesh: sp: 4 (over z), dp: 8 (over y, x, core).
Axes of the slice: x: 2, y: 2, z: 4, core: 2. Of those that a mesh axis runs over, the one named last changes fastest.
Arguments:
- inputs: bfloat16 [8, 512, 2048], P('dp', 'sp'), may hold values from -0.75 to 0.75
- queries: bfloat16 [8, 512, 1024], P('dp', 'sp'), may hold values from -18 to 18
- keys: bfloat16 [8, 512, 256], P('dp', 'sp'), may hold values from -18 to 18
- values: bfloat16 [8, 512, 256], P('dp', 'sp'), may hold values from -6 to 6
- out_grad: bfloat16 [8, 512, 1024], P('dp', 'sp'), may hold values from -144 to 144
- query_gain: float32 [64], replicated, may hold values from 0.4 to 6.5
- key_gain: float32 [64], replicated, may hold values from 0.4 to 6.5
- key_matrix: bfloat16 [2048, 256], P('dp'), may hold values from -0.125 to 0.125
- value_matrix: bfloat16 [2048, 256], P('dp'), may hold values from -0.125 to 0.125
Outputs:
- input_grad: bfloat16 [8, 512, 2048], P('dp', 'sp')
- query_grad: bfloat16 [8, 512, 1024], P('dp', 'sp')
- key_weight_grad: float32 [2048, 256], P('dp')
- value_weight_grad: float32 [2048, 256], P('dp')
All inputs are finite; a program needn't handle non-finite values.
Results may differ from a plain program's by a relative error of at most 0.024.
The roundings to bfloat16 on the way count: a program that leaves them out, or rounds other values in their place, can miss the bound.
Values may be sent and summed in bfloat16 or wider, within the bound.
A program may use at most 64 MiB of HBM per device.

v0:
```python
import jax
import jax.numpy as jnp
from jax import lax
from jax.sharding import PartitionSpec as P

QUERY_HEADS = 16
KEY_VALUE_HEADS = 4
HEAD_CHANNELS = 64
GRID = 64


rope_base = 10000.0
norm_eps = 0.5
score_scale = 0.125


def product(pattern, first_op, second_op):
    return jnp.einsum(pattern, first_op, second_op, preferred_element_type=jnp.float32)


def rotary_tables(token_length):
    position = jnp.arange(token_length, dtype=jnp.int32)
    grid_row = (position // GRID).astype(jnp.float32)
    grid_col = (position % GRID).astype(jnp.float32)
    half_pairs = HEAD_CHANNELS // 4
    inv_freq = rope_base ** (-jnp.arange(half_pairs, dtype=jnp.float32) / half_pairs)
    angles = jnp.concatenate([grid_row[:, None] * inv_freq, grid_col[:, None] * inv_freq], axis=1)
    return (jnp.cos(angles), jnp.sin(angles))


def rotate(vector, cos_tab, sin_tab):
    even_part = vector[..., 0::2]
    odd_part = vector[..., 1::2]
    turned = jnp.stack(
        [even_part * cos_tab - odd_part * sin_tab, even_part * sin_tab + odd_part * cos_tab],
        axis=-1,
    )
    return turned.reshape(vector.shape)


def rotate_back(cotangent, cos_tab, sin_tab):
    even_part = cotangent[..., 0::2]
    odd_part = cotangent[..., 1::2]
    turned = jnp.stack(
        [even_part * cos_tab + odd_part * sin_tab, odd_part * cos_tab - even_part * sin_tab],
        axis=-1,
    )
    return turned.reshape(cotangent.shape)


def inverse_rms(vector):
    return lax.rsqrt(jnp.mean(vector * vector, axis=-1, keepdims=True) + norm_eps)


def norm_back(vector, inv_scale, cotangent, gain_vec):
    weighted = cotangent * gain_vec
    inner_mean = jnp.mean(weighted * vector, axis=-1, keepdims=True)
    return inv_scale * (weighted - vector * inv_scale * inv_scale * inner_mean)


def head_grads(
    query_in, key_input, value_input, grad_in, query_gain, key_gain, cos_tab, sin_tab, block_rows
):
    token_length, groups, per_group, head_dim = query_in.shape
    cos_four = cos_tab[:, None, None, :]
    sin_four = sin_tab[:, None, None, :]
    cos_three = cos_tab[:, None, :]
    sin_three = sin_tab[:, None, :]
    query_f = query_in.astype(jnp.float32)
    query_inv = inverse_rms(query_f)
    query_rot = rotate(query_f * query_inv * query_gain, cos_four, sin_four).astype(jnp.bfloat16)
    key_f = key_input.astype(jnp.float32)
    key_inv = inverse_rms(key_f)
    key_rot = rotate(key_f * key_inv * key_gain, cos_three, sin_three).astype(jnp.bfloat16)
    num_blocks = token_length // block_rows
    query_blocks = query_rot.reshape(num_blocks, block_rows, groups, per_group, head_dim)
    grad_blocks = grad_in.reshape(num_blocks, block_rows, groups, per_group, head_dim)

    def attend_block(carried, pieces):
        key_acc, value_acc = carried
        query_piece, grad_piece = pieces
        scores = product("qgrd,cgd->grqc", query_piece, key_rot) * score_scale
        row_max = jnp.max(scores, axis=-1, keepdims=True)
        shifted = jnp.exp(scores - row_max)
        attn_prob = shifted / jnp.sum(shifted, axis=-1, keepdims=True)
        prob_low = attn_prob.astype(jnp.bfloat16)
        prob_grad = product("qgrd,cgd->grqc", grad_piece, value_input)
        row_dot = jnp.sum(attn_prob * prob_grad, axis=-1, keepdims=True)
        score_grad = (attn_prob * (prob_grad - row_dot) * score_scale).astype(jnp.bfloat16)
        dq_piece = product("grqc,cgd->qgrd", score_grad, key_rot)
        key_acc = key_acc + product("grqc,qgrd->cgd", score_grad, query_piece)
        value_acc = value_acc + product("grqc,qgrd->cgd", prob_low, grad_piece)
        return ((key_acc, value_acc), dq_piece)

    empty_acc = jnp.zeros((token_length, groups, head_dim), jnp.float32)
    (key_rot_grad, value_acc), query_rot_grad = lax.scan(
        attend_block, (empty_acc, empty_acc), (query_blocks, grad_blocks)
    )
    query_rot_grad = query_rot_grad.reshape(token_length, groups, per_group, head_dim)
    query_grad = norm_back(
        query_f, query_inv, rotate_back(query_rot_grad, cos_four, sin_four), query_gain
    ).astype(jnp.bfloat16)
    key_portion = norm_back(
        key_f, key_inv, rotate_back(key_rot_grad, cos_three, sin_three), key_gain
    ).astype(jnp.bfloat16)
    return (query_grad, key_portion, value_acc.astype(jnp.bfloat16))


def on_device(
    inputs, queries, keys, values, out_grad, query_gain, key_gain, key_matrix, value_matrix
):
    sp_count = lax.axis_size("sp")
    dp_count = lax.axis_size("dp")
    token_row_block = inputs.shape[1]
    token_length = token_row_block * sp_count
    local_heads = QUERY_HEADS // sp_count
    portion_heads = min(local_heads, QUERY_HEADS // KEY_VALUE_HEADS)
    kv_here = local_heads // portion_heads
    group_copies = QUERY_HEADS // KEY_VALUE_HEADS // portion_heads
    key_value_width = KEY_VALUE_HEADS * HEAD_CHANNELS
    key_positions = jnp.repeat(
        keys[0].reshape(token_row_block, KEY_VALUE_HEADS, HEAD_CHANNELS), group_copies, axis=1
    ).reshape(token_row_block, key_value_width * group_copies)
    value_positions = jnp.repeat(
        values[0].reshape(token_row_block, KEY_VALUE_HEADS, HEAD_CHANNELS), group_copies, axis=1
    ).reshape(token_row_block, key_value_width * group_copies)
    grad_heads, query_heads, key_heads, value_heads = (
        lax.all_to_all(out_grad[0], "sp", split_axis=1, concat_axis=0, tiled=True),
        lax.all_to_all(queries[0], "sp", split_axis=1, concat_axis=0, tiled=True),
        lax.all_to_all(key_positions, "sp", split_axis=1, concat_axis=0, tiled=True),
        lax.all_to_all(value_positions, "sp", split_axis=1, concat_axis=0, tiled=True),
    )
    cos_tab, sin_tab = rotary_tables(token_length)
    query_part, key_portion, value_portion = head_grads(
        query_heads.reshape(token_length, kv_here, portion_heads, HEAD_CHANNELS),
        key_heads.reshape(token_length, kv_here, HEAD_CHANNELS),
        value_heads.reshape(token_length, kv_here, HEAD_CHANNELS),
        grad_heads.reshape(token_length, kv_here, portion_heads, HEAD_CHANNELS),
        query_gain,
        key_gain,
        cos_tab,
        sin_tab,
        min(512, token_length),
    )
    query_tokens, key_token_rows, value_token_rows = (
        lax.all_to_all(
            query_part.reshape(token_length, local_heads * HEAD_CHANNELS),
            "sp",
            split_axis=0,
            concat_axis=1,
            tiled=True,
        ),
        lax.all_to_all(
            key_portion.reshape(token_length, kv_here * HEAD_CHANNELS),
            "sp",
            split_axis=0,
            concat_axis=1,
            tiled=True,
        ),
        lax.all_to_all(
            value_portion.reshape(token_length, kv_here * HEAD_CHANNELS),
            "sp",
            split_axis=0,
            concat_axis=1,
            tiled=True,
        ),
    )
    key_gradient = (
        key_token_rows.reshape(token_row_block, KEY_VALUE_HEADS, group_copies, HEAD_CHANNELS)
        .astype(jnp.float32)
        .sum(axis=2)
        .astype(jnp.bfloat16)
    )
    value_gradient = (
        value_token_rows.reshape(token_row_block, KEY_VALUE_HEADS, group_copies, HEAD_CHANNELS)
        .astype(jnp.float32)
        .sum(axis=2)
        .astype(jnp.bfloat16)
    )
    projection_gradient = jnp.concatenate(
        [
            key_gradient.reshape(token_row_block, key_value_width),
            value_gradient.reshape(token_row_block, key_value_width),
        ],
        axis=1,
    )
    joined_weight = jnp.concatenate([key_matrix, value_matrix], axis=1)
    input_grad = lax.dot_general(
        projection_gradient,
        lax.all_gather(joined_weight, "dp", axis=0, tiled=True),
        (((1,), (1,)), ((), ())),
        preferred_element_type=jnp.float32,
    ).astype(jnp.bfloat16)
    token_in = inputs[0]
    width = inputs.shape[2]
    row_share = width // (sp_count * dp_count)
    permuted = (
        token_in.reshape(token_row_block, dp_count, sp_count, row_share)
        .transpose(0, 2, 1, 3)
        .reshape(token_row_block, width)
    )
    share_cols = lax.all_to_all(permuted, "sp", split_axis=1, concat_axis=0, tiled=True)
    all_grads = lax.all_gather(projection_gradient, "sp", axis=0, tiled=True)
    grad_piece = lax.psum_scatter(
        lax.dot_general(
            share_cols, all_grads, (((0,), (0,)), ((), ())), preferred_element_type=jnp.float32
        ).astype(jnp.bfloat16),
        "dp",
        scatter_dimension=0,
        tiled=True,
    ).astype(jnp.float32)
    weight_grad = lax.all_gather(grad_piece, "sp", axis=0, tiled=True)
    return (
        input_grad[None],
        query_tokens[None],
        weight_grad[:, :key_value_width],
        weight_grad[:, key_value_width:],
    )


def solution(mesh):
    return jax.shard_map(
        on_device,
        mesh=mesh,
        in_specs=(
            P("dp", "sp", None),
            P("dp", "sp", None),
            P("dp", "sp", None),
            P("dp", "sp", None),
            P("dp", "sp", None),
            P(),
            P(),
            P("dp", None),
            P("dp", None),
        ),
        out_specs=(P("dp", "sp", None), P("dp", "sp", None), P("dp", None), P("dp", None)),
        check_vma=False,
    )
```

profile of v0, /device:TPU:0, one launch (start us, length us, event | category | flops | bytes accessed | tf_op | source)
XLA Modules:
  0.0 183.9 jit_solution(14497211045874740525)
XLA Ops:
  8.8 6.3 %all-to-all-start = ((bf16[128,4,64]{0,2,1:T(8,128)(2,1)}), bf16[128,4,64]{0,2,1:T(8,128)(2,1)S(1)}, u32[]{:S(2)}, u32[]{:S(2)}) async-start(bf16[128,4,64]{0,2,1:T(8,128)(2,1)} %bitcast), calls=%async_computation | async-start | bytes 131072 | tf_op jit(solution)/shard_map/all_to_all | solution.py:130
  15.1 1.8 copy.143
  16.9 1.8 copy.150
  20.8 4.9 %all-to-all-start.2 = ((bf16[128,4,64]{0,2,1:T(8,128)(2,1)}), bf16[128,4,64]{0,2,1:T(8,128)(2,1)S(1)}, u32[]{:S(2)}, u32[]{:S(2)}) async-start(bf16[128,4,64]{0,2,1:T(8,128)(2,1)} %bitcast.21), calls=%async_computation.2 | async-start | bytes 131072 | tf_op jit(solution)/shard_map/all_to_all | solution.py:131
  26.5 5.0 %all-to-all-done.2 = bf16[128,4,64]{0,2,1:T(8,128)(2,1)S(1)} async-done(((bf16[128,4,64]{0,2,1:T(8,128)(2,1)}), bf16[128,4,64]{0,2,1:T(8,128)(2,1)S(1)}, u32[]{:S(2)}, u32[]{:S(2)}) %all-to-all-start.2) | async-done | bytes 65568 | tf_op jit(solution)/shard_map/all_to_all | solution.py:131
  31.5 3.4 %all-to-all-start.1 = ((bf16[128,4,256]{0,2,1:T(8,128)(2,1)}), bf16[128,4,256]{0,2,1:T(8,128)(2,1)S(1)}, u32[]{:S(2)}, u32[]{:S(2)}) async-start(bf16[128,4,256]{0,2,1:T(8,128)(2,1)} %bitcast.2), calls=%async_computation.1 | async-start | bytes 524288 | tf_op jit(solution)/shard_map/all_to_all | solution.py:129
  36.1 5.6 %all-to-all-done.1 = bf16[128,4,256]{0,2,1:T(8,128)(2,1)S(1)} async-done(((bf16[128,4,256]{0,2,1:T(8,128)(2,1)}), bf16[128,4,256]{0,2,1:T(8,128)(2,1)S(1)}, u32[]{:S(2)}, u32[]{:S(2)}) %all-to-all-start.1) | async-done | bytes 262176 | tf_op jit(solution)/shard_map/all_to_all | solution.py:129
  41.6 3.4 %all-to-all-start.3 = ((bf16[128,4,256]{0,2,1:T(8,128)(2,1)}), bf16[128,4,256]{0,2,1:T(8,128)(2,1)S(1)}, u32[]{:S(2)}, u32[]{:S(2)}) async-start(bf16[128,4,256]{0,2,1:T(8,128)(2,1)} %bitcast.23), calls=%async_computation.3 | async-start | bytes 524288 | tf_op jit(solution)/shard_map/all_to_all | solution.py:128
  46.2 5.7 %all-to-all-done.3 = bf16[128,4,256]{0,2,1:T(8,128)(2,1)S(1)} async-done(((bf16[128,4,256]{0,2,1:T(8,128)(2,1)}), bf16[128,4,256]{0,2,1:T(8,128)(2,1)S(1)}, u32[]{:S(2)}, u32[]{:S(2)}) %all-to-all-start.3) | async-done | bytes 262176 | tf_op jit(solution)/shard_map/all_to_all | solution.py:128
  60.1 3.4 %all-to-all-start.4 = ((bf16[4,128,64]{1,2,0:T(8,128)(2,1)}), bf16[4,128,64]{1,2,0:T(8,128)(2,1)S(1)}, u32[]{:S(2)}, u32[]{:S(2)}) async-start(bf16[4,128,64]{1,2,0:T(8,128)(2,1)} %multiply_convert_fusion), calls=%async_computation.4 | async-start | bytes 131072 | tf_op jit(solution)/shard_map/all_to_all | solution.py:153
  63.6 3.2 %fusion.19 = bf16[512,1,64]{0,2,1:T(8,128)(2,1)S(1)} fusion(bf16[512,4,64]{0,2,1:T(8,128)(2,1)} %copy-done.5, f32[512,512,4,1]{1,0,3,2:T(8,128)} %copy-done, f32[4,512]{1,0:T(4,128)} %copy-done.6, f32[4,512]{1,0:T(4,128)S(1)} %get-tuple-element.74), kind=kOutput, calls=%fused_computation.24 | convolution fusion | flops 138444800 | bytes 4538368 | tf_op jit(solution)/shard_map/while/body/eval_jaxpr/grqc,qgrd->cgd/dot_general | solution.py:18
  67.4 1.9 %all-to-all-done.4 = bf16[4,128,64]{1,2,0:T(8,128)(2,1)S(1)} async-done(((bf16[4,128,64]{1,2,0:T(8,128)(2,1)}), bf16[4,128,64]{1,2,0:T(8,128)(2,1)S(1)}, u32[]{:S(2)}, u32[]{:S(2)}) %all-to-all-start.4) | async-done | bytes 65568 | tf_op jit(solution)/shard_map/all_to_all | solution.py:153
  69.9 3.9 %all-to-all-start.5 = ((bf16[4,128,64]{1,2,0:T(8,128)(2,1)}), bf16[4,128,64]{1,2,0:T(8,128)(2,1)}, u32[]{:S(2)}, u32[]{:S(2)}) async-start(bf16[4,128,64]{1,2,0:T(8,128)(2,1)} %copy.157), calls=%async_computation.5 | async-start | bytes 131072 | tf_op jit(solution)/shard_map/all_to_all | solution.py:160
  76.0 3.6 %all-to-all-done.5 = bf16[4,128,64]{1,2,0:T(8,128)(2,1)} async-done(((bf16[4,128,64]{1,2,0:T(8,128)(2,1)}), bf16[4,128,64]{1,2,0:T(8,128)(2,1)}, u32[]{:S(2)}, u32[]{:S(2)}) %all-to-all-start.5) | async-done | bytes 65568 | tf_op jit(solution)/shard_map/all_to_all | solution.py:160
  79.6 4.1 %all-to-all-start.7 = ((bf16[128,4,512]{0,2,1:T(8,128)(2,1)}), bf16[128,4,512]{0,2,1:T(8,128)(2,1)}, u32[]{:S(2)}, u32[]{:S(2)}) async-start(bf16[128,4,512]{0,2,1:T(8,128)(2,1)} %bitcast.56), calls=%async_computation.7 | async-start | bytes 1048576 | tf_op jit(solution)/shard_map/all_to_all | solution.py:202
  84.7 19.0 %all_gather.10 = bf16[512,512]{0,1:T(8,128)(2,1)S(1)} all-gather(bf16[128,512]{0,1:T(8,128)(2,1)S(1)} %pad_maximum_fusion.4), channel_id=1, replica_groups=mesh['sp'=4,'dp'=8] {'sp'}, dimensions={0}, use_global_device_ids=true | all-gather | bytes 655360 | tf_op jit(solution)/shard_map/all_gather | solution.py:203
  103.7 2.0 %copy.171 = bf16[4,128,512]{2,1,0:T(8,128)(2,1)} copy(bf16[4,128,512]{1,2,0:T(8,128)(2,1)} %bitcast.57) | data formatting | bytes 1048576 | tf_op jit(solution)/shard_map/all_to_all | solution.py:202
  105.8 2.3 %fusion.12 = bf16[512,512]{0,1:T(8,128)(2,1)} fusion(bf16[512,512]{0,1:T(8,128)(2,1)S(1)} %all_gather.10, bf16[512,512]{1,0:T(8,128)(2,1)} %bitcast.182), kind=kOutput, calls=%fused_computation.20 | convolution fusion | flops 268697600 | bytes 1572864 | tf_op jit(solution)/shard_map/dot_general | solution.py:205
  108.0 2.0 %copy.178 = bf16[512,512]{1,0:T(8,128)(2,1)} copy(bf16[512,512]{0,1:T(8,128)(2,1)} %fusion.12) | data formatting | bytes 1048576
  117.9 10.3 %all_to_all.113 = bf16[4,128,256]{1,2,0:T(8,128)(2,1)S(1)} all-to-all(bf16[4,128,256]{1,2,0:T(8,128)(2,1)S(1)} %fusion.25), channel_id=1, replica_groups=mesh['sp'=4,'dp'=8] {'sp'}, dimensions={0} | all-to-all | bytes 524288 | tf_op jit(solution)/shard_map/all_to_all | solution.py:146
  129.0 15.1 %reduce-scatter.4.cloned.1.call-done = bf16[64,512]{1,0:T(8,128)(2,1)} async-done(((bf16[512,512]{1,0:T(8,128)(2,1)}), bf16[64,512]{1,0:T(8,128)(2,1)}) %reduce-scatter.4.cloned.1.call-update) | async-done | bytes 65552 | tf_op jit(solution)/shard_map/reduce_scatter | solution.py:204
  145.0 15.2 %all_gather.11 = f32[256,512]{1,0:T(8,128)S(1)} all-gather(f32[64,512]{1,0:T(8,128)S(1)} %convert_element_type.220), channel_id=1, replica_groups=mesh['sp'=4,'dp'=8] {'sp'}, dimensions={0}, use_global_device_ids=true | all-gather | bytes 655360 | tf_op jit(solution)/shard_map/all_gather | solution.py:212
  161.0 12.8 %all-gather.2.cloned.1.call-done = bf16[2048,512]{1,0:T(8,128)(2,1)} async-done(((bf16[256,512]{1,0:T(8,128)(2,1)}), bf16[2048,512]{1,0:T(8,128)(2,1)}) %all-gather.2.cloned.1.call-update) | async-done | bytes 2097168 | tf_op jit(solution)/shard_map/all_gather | solution.py:190
  173.9 3.2 %fusion.7 = bf16[1,128,2048]{2,1,0:T(8,128)(2,1)} fusion(bf16[2048,512]{1,0:T(8,128)(2,1)} %all-gather.2.cloned.1.call-done, bf16[128,256]{0,1:T(8,128)(2,1)} %bitcast.43, bf16[128,256]{0,1:T(8,128)(2,1)S(1)} %bitcast.192), kind=kOutput, calls=%fused_computation.13 | convolution fusion | flops 268959744 | bytes 2752512 | tf_op jit(solution)/shard_map/dot_general | solution.py:188
  (98 shorter events, 29.4 us)
Async XLA Ops:
  7.2 38.6 %copy-start.7 = (f32[64]{0:T(128)S(1)}, f32[64]{0:T(128)}, u32[]{:S(2)}) copy-start(f32[64]{0:T(128)} %param.14) | copy-start | bytes 772
  8.8 12.1 %all-to-all-start = ((bf16[128,4,64]{0,2,1:T(8,128)(2,1)}), bf16[128,4,64]{0,2,1:T(8,128)(2,1)S(1)}, u32[]{:S(2)}, u32[]{:S(2)}) async-start(bf16[128,4,64]{0,2,1:T(8,128)(2,1)} %bitcast), calls=%async_computation | async-start | bytes 131072 | tf_op jit(solution)/shard_map/all_to_all | solution.py:130
  20.8 10.6 %all-to-all-start.2 = ((bf16[128,4,64]{0,2,1:T(8,128)(2,1)}), bf16[128,4,64]{0,2,1:T(8,128)(2,1)S(1)}, u32[]{:S(2)}, u32[]{:S(2)}) async-start(bf16[128,4,64]{0,2,1:T(8,128)(2,1)} %bitcast.21), calls=%async_computation.2 | async-start | bytes 131072 | tf_op jit(solution)/shard_map/all_to_all | solution.py:131
  31.5 10.2 %all-to-all-start.1 = ((bf16[128,4,256]{0,2,1:T(8,128)(2,1)}), bf16[128,4,256]{0,2,1:T(8,128)(2,1)S(1)}, u32[]{:S(2)}, u32[]{:S(2)}) async-start(bf16[128,4,256]{0,2,1:T(8,128)(2,1)} %bitcast.2), calls=%async_computation.1 | async-start | bytes 524288 | tf_op jit(solution)/shard_map/all_to_all | solution.py:129
  36.0 16.5 %copy-start.3 = (bf16[512,1,32]{0,2,1:T(8,128)(2,1)}, bf16[512,1,32]{0,2,1:T(8,128)(2,1)S(1)}, u32[]{:S(2)}) copy-start(bf16[512,1,32]{0,2,1:T(8,128)(2,1)S(1)} %get-tuple-element.62) | copy-start | bytes 98308
  36.0 16.5 %copy-start.4 = (bf16[512,1,32]{0,2,1:T(8,128)(2,1)}, bf16[512,1,32]{0,2,1:T(8,128)(2,1)S(1)}, u32[]{:S(2)}) copy-start(bf16[512,1,32]{0,2,1:T(8,128)(2,1)S(1)} %get-tuple-element.63) | copy-start | bytes 98308
  41.6 10.2 %all-to-all-start.3 = ((bf16[128,4,256]{0,2,1:T(8,128)(2,1)}), bf16[128,4,256]{0,2,1:T(8,128)(2,1)S(1)}, u32[]{:S(2)}, u32[]{:S(2)}) async-start(bf16[128,4,256]{0,2,1:T(8,128)(2,1)} %bitcast.23), calls=%async_computation.3 | async-start | bytes 524288 | tf_op jit(solution)/shard_map/all_to_all | solution.py:128
  52.1 1.8 copy-start.5
  53.2 2.0 %copy-start = (f32[512,512,4,1]{1,0,3,2:T(8,128)}, f32[512,512,4,1]{1,0,3,2:T(8,128)S(1)}, u32[]{:S(2)}) copy-start(f32[512,512,4,1]{1,0,3,2:T(8,128)S(1)} %get-tuple-element.75) | copy-start | bytes 12582916
  54.0 1.3 copy-start.6
  60.1 9.2 %all-to-all-start.4 = ((bf16[4,128,64]{1,2,0:T(8,128)(2,1)}), bf16[4,128,64]{1,2,0:T(8,128)(2,1)S(1)}, u32[]{:S(2)}, u32[]{:S(2)}) async-start(bf16[4,128,64]{1,2,0:T(8,128)(2,1)} %multiply_convert_fusion), calls=%async_computation.4 | async-start | bytes 131072 | tf_op jit(solution)/shard_map/all_to_all | solution.py:153
  69.3 0.6 copy-start.1
  69.9 9.7 %all-to-all-start.5 = ((bf16[4,128,64]{1,2,0:T(8,128)(2,1)}), bf16[4,128,64]{1,2,0:T(8,128)(2,1)}, u32[]{:S(2)}, u32[]{:S(2)}) async-start(bf16[4,128,64]{1,2,0:T(8,128)(2,1)} %copy.157), calls=%async_computation.5 | async-start | bytes 131072 | tf_op jit(solution)/shard_map/all_to_all | solution.py:160
  75.1 36.9 %copy-start.8 = (f32[64]{0:T(128)S(1)}, f32[64]{0:T(128)}, u32[]{:S(2)}) copy-start(f32[64]{0:T(128)} %param.14) | copy-start | bytes 772
  79.6 24.1 %all-to-all-start.7 = ((bf16[128,4,512]{0,2,1:T(8,128)(2,1)}), bf16[128,4,512]{0,2,1:T(8,128)(2,1)}, u32[]{:S(2)}, u32[]{:S(2)}) async-start(bf16[128,4,512]{0,2,1:T(8,128)(2,1)} %bitcast.56), calls=%async_computation.7 | async-start | bytes 1048576 | tf_op jit(solution)/shard_map/all_to_all | solution.py:202
  83.8 60.3 %reduce-scatter.4.cloned.1.call-start = ((), (), s32[]{:S(2)}) async-start(), calls=%async_computation.10 | async-start | bytes 589824 | tf_op jit(solution)/shard_map/reduce_scatter | solution.py:204
  110.1 63.8 %all-gather.2.cloned.1.call-start = ((), (), s32[]{:S(2)}) async-start(), calls=%async_computation.9 | async-start | bytes 2359296 | tf_op jit(solution)/shard_map/all_gather | solution.py:190
  116.5 57.4 %copy-start.2 = (bf16[4,128,64]{1,2,0:T(8,128)(2,1)S(1)}, bf16[4,128,64]{1,2,0:T(8,128)(2,1)}, u32[]{:S(2)}) copy-start(bf16[4,128,64]{1,2,0:T(8,128)(2,1)} %copy-done.1) | copy-start | bytes 196612
Sparse Core Ops, SparseCore 0:
  110.2 33.8 reduce-scatter.3
  146.0 27.7 all-gather.1
where the time goes:
time: 185 us; the launch traced here: 184 us
  waiting for transfers between devices  49.9 us (27%)
  blocking collectives  44.5 us (24%)
  starting transfers between devices  29.8 us (16%)
  local copies, waits for them, and re-layouts  20.9 us (11%)
  between operations  14.5 us (8%)
  matrix products  12.8 us (7%)
  other arithmetic  11.5 us (6%)
    all_gather x1, blocking collectives, on_device(): all_grads = lax.all_gather(projection_gradient, 'sp', axis=0, tiled=True)  19 us
    all_gather x1, blocking collectives, on_device(): weight_grad = lax.all_gather(grad_piece, 'sp', axis=0, tiled=True)  15.2 us
    reduce_scatter x1, waiting for transfers between devices, on_device(): lax.psum_scatter(lax.dot_general(share_cols, all_grads, (((0,), (0,)), ((...  15.1 us
    all_gather x1, waiting for transfers between devices, on_device(): lax.all_gather(joined_weight, 'dp', axis=0, tiled=True)  12.8 us
    unnamed x25, local copies, waits for them, and re-layouts  11.6 us
    all_to_all x1, blocking collectives, on_device(): lax.all_to_all(query_part.reshape(token_length, local_heads * HEAD_CHANNE...  10.3 us
    dot_general x5, matrix products, product(): jnp.einsum(pattern, first_op, second_op, preferred_element_type=jnp.float32)  7.27 us
    all_to_all x1, starting transfers between devices, on_device(): lax.all_to_all(key_positions, 'sp', split_axis=1, concat_axis=0, tiled=True)  6.35 us
  transfers between devices with their start and end apart: 9, of which 8 were waited for; matrix products, arithmetic and copies ran while one was open for 14% of the time, Pallas kernels for 0%

commit v1 on v0

--- a/solution.py
+++ b/solution.py
@@ -1,6 +1,11 @@
+import functools
+
 import jax
 import jax.numpy as jnp
+import numpy as np
 from jax import lax
+from jax.experimental import pallas as pl
+from jax.experimental.pallas import tpu as pltpu
 from jax.sharding import PartitionSpec as P
 
 QUERY_HEADS = 16
@@ -218,9 +223,369 @@
     )
 
 
+LANES = 128
+MESH = pl.DeviceIdType.MESH
+F32 = jnp.float32
+BF16 = jnp.bfloat16
+
+
+def pair_tables(token_length):
+    position = np.arange(token_length)
+    half_pairs = HEAD_CHANNELS // 4
+    inv_freq = (rope_base ** (-np.arange(half_pairs) / half_pairs)).astype(np.float32)
+    row = (position // GRID).astype(np.float32)
+    col = (position % GRID).astype(np.float32)
+    angles = np.concatenate([row[:, None] * inv_freq, col[:, None] * inv_freq], axis=1)
+    cos_tab = np.repeat(np.cos(angles), 2, axis=1)
+    sin_tab = np.repeat(np.sin(angles), 2, axis=1)
+    sin_tab[:, 0::2] *= -1.0
+    return (
+        np.tile(cos_tab, (1, 2)).astype(np.float32),
+        np.tile(sin_tab, (1, 2)).astype(np.float32),
+    )
+
+
+def swap_pairs(x):
+    lane = lax.broadcasted_iota(jnp.int32, x.shape, 1)
+    return jnp.where(lane % 2 == 0, pltpu.roll(x, LANES - 1, 1), pltpu.roll(x, 1, 1))
+
+
+def head_mean(z):
+    row = lax.broadcasted_iota(jnp.int32, (LANES, LANES), 0) // HEAD_CHANNELS
+    col = lax.broadcasted_iota(jnp.int32, (LANES, LANES), 1) // HEAD_CHANNELS
+    ones = jnp.where(row == col, 1.0, 0.0).astype(BF16)
+    high = z.astype(BF16)
+    low = (z - high.astype(F32)).astype(BF16)
+    total = jnp.dot(high, ones, preferred_element_type=F32)
+    total = total + jnp.dot(low, ones, preferred_element_type=F32)
+    return total * (1.0 / HEAD_CHANNELS)
+
+
+def norm_rotate(x, gain, cos_tab, sin_tab):
+    inv = lax.rsqrt(head_mean(x * x) + norm_eps)
+    y = x * inv * gain
+    return y * cos_tab + swap_pairs(y) * sin_tab
+
+
+def norm_rotate_back(x, cotangent, gain, cos_tab, sin_tab):
+    turned = cotangent * cos_tab - swap_pairs(cotangent) * sin_tab
+    inv = lax.rsqrt(head_mean(x * x) + norm_eps)
+    weighted = turned * gain
+    return inv * (weighted - x * (inv * inv * head_mean(weighted * x)))
+
+
+def contract(a, b, dims):
+    return lax.dot_general(a, b, (dims, ((), ())), preferred_element_type=F32)
+
+
+def step_kernel(
+    n, dp,
+    x_hbm, q_hbm, k_hbm, v_hbm, do_hbm, qg_ref, kg_ref, km_hbm, vm_hbm, cos_hbm, sin_hbm,
+    dx_ref, dq_ref, kw_ref, vw_ref,
+    q_buf, do_buf, cos_buf, sin_buf, k_all, v_all, x_all, wk_all, wv_all,
+    q_st, do_st, k_st, v_st, dq_acc, part, got, g_all, x_t, wg_part, wg_got, fin_all,
+    local_sem, kv_send, kv_recv, x_send, x_recv, w_send, w_recv, w_fsend,
+    p_send, p_recv, g_send, g_recv, g_fsend, r_send, r_recv, f_send, f_recv,
+):
+    me = lax.axis_index("sp")
+    md = lax.axis_index("dp")
+    rows, q_width = q_buf.shape
+    kv_width = k_all.shape[2]
+    share = x_all.shape[2]
+    kv_heads = kv_width // HEAD_CHANNELS
+    per_group = q_width // kv_width
+    mate = md + 1 - 2 * (md % 2)
+    pairs = dp // 2
+
+    def sp_peer(o):
+        return lax.rem(me + o, n)
+
+    def sp_from(o):
+        return lax.rem(me - o + n, n)
+
+    def dp_peer(o):
+        return lax.rem(md + o, dp)
+
+    def dp_from(o):
+        return lax.rem(md - o + dp, dp)
+
+    barrier = pltpu.get_barrier_semaphore()
+    for o in range(1, n):
+        pl.semaphore_signal(barrier, inc=1, device_id={"sp": sp_peer(o)}, device_id_type=MESH)
+    for o in range(1, dp):
+        pl.semaphore_signal(barrier, inc=1, device_id={"dp": dp_peer(o)}, device_id_type=MESH)
+
+    def columns(d):
+        return pl.ds(pl.multiple_of(d * share, share), share)
+
+    local = [
+        pltpu.make_async_copy(src, dst, local_sem.at[i])
+        for i, (src, dst) in enumerate([
+            (q_hbm, q_buf), (do_hbm, do_buf), (cos_hbm, cos_buf), (sin_hbm, sin_buf),
+            (k_hbm, k_all.at[me]), (v_hbm, v_all.at[me]),
+            (x_hbm.at[:, columns(md)], x_all.at[md]),
+            (km_hbm, wk_all.at[md]), (vm_hbm, wv_all.at[md]),
+        ])
+    ]
+    for copy in local:
+        copy.start()
+
+    def remote(src, dst, send, recv, where):
+        return pltpu.make_async_remote_copy(
+            src_ref=src, dst_ref=dst, send_sem=send, recv_sem=recv,
+            device_id=where, device_id_type=MESH,
+        )
+
+    pl.semaphore_wait(barrier, n + dp - 2)
+
+    sends = []
+
+    def send(*args):
+        copy = remote(*args)
+        copy.start()
+        sends.append(copy)
+
+    def arrived(dst, recv):
+        remote(dst, dst, recv, recv, {"sp": me}).wait_recv()
+
+    order = sorted(range(1, n), key=lambda o: -min(o, n - o))
+    for kind, (src, dst) in enumerate([(k_hbm, k_all), (v_hbm, v_all)]):
+        for o in order:
+            send(src, dst.at[me], kv_send.at[kind, o], kv_recv.at[kind, me], {"sp": sp_peer(o)})
+    weights = [(km_hbm, wk_all), (vm_hbm, wv_all)]
+    for kind, (src, dst) in enumerate(weights):
+        for o in range(2, dp, 2):
+            send(src, dst.at[md], w_send.at[kind, o], w_recv.at[kind, md], {"dp": dp_peer(o)})
+        send(src, dst.at[md], w_send.at[kind, 1], w_recv.at[kind, md], {"dp": mate})
+    for o in range(1, dp):
+        send(x_hbm.at[:, columns(dp_peer(o))], x_all.at[md], x_send.at[o], x_recv.at[md],
+             {"dp": dp_peer(o)})
+
+    for copy in local:
+        copy.wait()
+
+    my_rows = pl.ds(pl.multiple_of(me * rows, rows), rows)
+    cos_own = cos_buf[my_rows, :]
+    sin_own = sin_buf[my_rows, :]
+    q_gain = qg_ref[...]
+    k_gain = kg_ref[...]
+
+    for c in range(q_width // LANES):
+        lanes = pl.ds(c * LANES, LANES)
+        turned = norm_rotate(q_buf[:, lanes].astype(F32), q_gain, cos_own, sin_own).astype(BF16)
+        grads = do_buf[:, lanes]
+        for a in range(2):
+            h = 2 * c + a
+            to = pl.ds((h % per_group) * rows, rows)
+            half = slice(a * HEAD_CHANNELS, (a + 1) * HEAD_CHANNELS)
+            q_st[h // per_group, to, :] = turned[:, half]
+            do_st[h // per_group, to, :] = grads[:, half]
+
+    def stack_keys(src):
+        at = pl.ds(pl.multiple_of(src * rows, rows), rows)
+        for c in range(kv_width // LANES):
+            lanes = pl.ds(c * LANES, LANES)
+            turned = norm_rotate(
+                k_all[src, :, lanes].astype(F32), k_gain, cos_buf[at, :], sin_buf[at, :]
+            ).astype(BF16)
+            vals = v_all[src, :, lanes]
+            for a in range(2):
+                half = slice(a * HEAD_CHANNELS, (a + 1) * HEAD_CHANNELS)
+                k_st[2 * c + a, at, :] = turned[:, half]
+                v_st[2 * c + a, at, :] = vals[:, half]
+
+    stack_keys(me)
+    for o in range(1, n):
+        src = sp_from(o)
+        arrived(k_all.at[src], kv_recv.at[0, src])
+        arrived(v_all.at[src], kv_recv.at[1, src])
+        stack_keys(src)
+
+    def attend(g):
+        qs = q_st[g]
+        dos = do_st[g]
+        ks = k_st[g]
+        vs = v_st[g]
+        scores = contract(ks, qs, ((1,), (1,))) * score_scale
+        shifted = jnp.exp(scores - jnp.max(scores, axis=0, keepdims=True))
+        prob = shifted * (1.0 / jnp.sum(shifted, axis=0, keepdims=True))
+        value_part = contract(prob.astype(BF16), dos, ((1,), (0,)))
+        prob_grad = contract(vs, dos, ((1,), (1,)))
+        row_dot = jnp.sum(prob * prob_grad, axis=0, keepdims=True)
+        score_grad = (prob * (prob_grad - row_dot) * score_scale).astype(BF16)
+        key_part = contract(score_grad, qs, ((1,), (0,)))
+        dq_t = contract(ks, score_grad, ((0,), (0,)))
+        for r in range(0, per_group, 2):
+            both = jnp.concatenate(
+                [dq_t[:, r * rows:(r + 1) * rows], dq_t[:, (r + 1) * rows:(r + 2) * rows]], axis=0
+            )
+            head = g * per_group + r
+            dq_acc[:, head * HEAD_CHANNELS:head * HEAD_CHANNELS + LANES] = both.T
+        return key_part, value_part
+
+    for c in range(kv_heads // 2):
+        key_low, value_low = attend(2 * c)
+        key_high, value_high = attend(2 * c + 1)
+        both = jnp.concatenate([key_low, key_high, value_low, value_high], axis=1).astype(BF16)
+        for j in range(n):
+            part[c, j] = both[j * rows:(j + 1) * rows, :]
+        for o in order:
+            send(part.at[c, sp_peer(o)], got.at[c, me], p_send.at[c, o], p_recv.at[c, me],
+                 {"sp": sp_peer(o)})
+
+    for kind, (_, dst) in enumerate(weights):
+        for o in range(2, dp, 2):
+            src = dp_from(o)
+            arrived(dst.at[src], w_recv.at[kind, src])
+            send(dst.at[src], dst.at[src], w_fsend.at[kind, o], w_recv.at[kind, src], {"dp": mate})
+
+    for c in range(q_width // LANES):
+        lanes = pl.ds(c * LANES, LANES)
+        dq_ref[:, lanes] = norm_rotate_back(
+            q_buf[:, lanes].astype(F32), dq_acc[:, lanes], q_gain, cos_own, sin_own
+        ).astype(BF16)
+
+    for o in range(dp):
+        src = dp_from(o)
+        if o:
+            arrived(x_all.at[src], x_recv.at[src])
+        x_t[src] = x_all[src].T
+
+    for c in range(kv_heads // 2):
+        total = part[c, me].astype(F32)
+        for o in range(1, n):
+            src = sp_from(o)
+            arrived(got.at[c, src], p_recv.at[c, src])
+            total = total + got[c, src].astype(F32)
+        lanes = pl.ds(c * LANES, LANES)
+        g_all[md, :, lanes] = norm_rotate_back(
+            k_all[me, :, lanes].astype(F32), total[:, :LANES], k_gain, cos_own, sin_own
+        ).astype(BF16)
+        g_all[md, :, pl.ds(kv_width + c * LANES, LANES)] = total[:, LANES:].astype(BF16)
+    for o in range(2, dp, 2):
+        send(g_all.at[md], g_all.at[md], g_send.at[o], g_recv.at[md], {"dp": dp_peer(o)})
+    send(g_all.at[md], g_all.at[md], g_send.at[1], g_recv.at[md], {"dp": mate})
+
+    own = g_all[md]
+    wgrad = contract(x_t[md], own, ((1,), (0,)))
+
+    def project(src):
+        out = contract(own[:, :kv_width], wk_all[src], ((1,), (1,)))
+        out = out + contract(own[:, kv_width:], wv_all[src], ((1,), (1,)))
+        dx_ref[:, columns(src)] = out.astype(BF16)
+
+    project(md)
+    for o in range(2, dp, 2):
+        project(dp_from(o))
+    for o in range(2, dp, 2):
+        src = dp_from(o)
+        arrived(g_all.at[src], g_recv.at[src])
+        send(g_all.at[src], g_all.at[src], g_fsend.at[o], g_recv.at[src], {"dp": mate})
+        wgrad = wgrad + contract(x_t[src], g_all[src], ((1,), (0,)))
+    for o in range(0, dp, 2):
+        src = lax.rem(mate - o + dp, dp)
+        arrived(g_all.at[src], g_recv.at[src])
+        wgrad = wgrad + contract(x_t[src], g_all[src], ((1,), (0,)))
+
+    piece = share // n
+    for j in range(n):
+        wg_part[j] = wgrad[j * piece:(j + 1) * piece, :].astype(BF16)
+    for o in order:
+        send(wg_part.at[sp_peer(o)], wg_got.at[me], r_send.at[o], r_recv.at[me],
+             {"sp": sp_peer(o)})
+    for o in range(0, dp, 2):
+        src = lax.rem(mate - o + dp, dp)
+        for kind, (_, dst) in enumerate(weights):
+            arrived(dst.at[src], w_recv.at[kind, src])
+        project(src)
+    total = wg_part[me].astype(F32)
+    for o in range(1, n):
+        src = sp_from(o)
+        arrived(wg_got.at[src], r_recv.at[src])
+        total = total + wg_got[src].astype(F32)
+    fin_all[me] = total.astype(BF16)
+    for o in order:
+        send(fin_all.at[me], fin_all.at[me], f_send.at[o], f_recv.at[me], {"sp": sp_peer(o)})
+    for o in range(n):
+        src = sp_from(o)
+        if o:
+            arrived(fin_all.at[src], f_recv.at[src])
+        at = pl.ds(pl.multiple_of(src * piece, piece), piece)
+        kw_ref[at, :] = fin_all[src, :, :kv_width].astype(F32)
+        vw_ref[at, :] = fin_all[src, :, kv_width:].astype(F32)
+    for copy in sends:
+        copy.wait_send()
+
+
+def kernel_step(
+    n, dp, inputs, queries, keys, values, out_grad, query_gain, key_gain, key_matrix, value_matrix
+):
+    rows, width = inputs.shape[1:]
+    q_width = queries.shape[2]
+    kv_width = keys.shape[2]
+    length = rows * n
+    share = width // dp
+    kv_heads = kv_width // HEAD_CHANNELS
+    stack = rows * (q_width // kv_width)
+    cos_tab, sin_tab = pair_tables(length)
+    vmem = functools.partial(pltpu.VMEM)
+    dma = pltpu.SemaphoreType.DMA
+    scratch = [
+        vmem((rows, q_width), BF16), vmem((rows, q_width), BF16),
+        vmem((length, LANES), F32), vmem((length, LANES), F32),
+        vmem((n, rows, kv_width), BF16), vmem((n, rows, kv_width), BF16),
+        vmem((dp, rows, share), BF16),
+        vmem((dp, share, kv_width), BF16), vmem((dp, share, kv_width), BF16),
+        vmem((kv_heads, stack, HEAD_CHANNELS), BF16), vmem((kv_heads, stack, HEAD_CHANNELS), BF16),
+        vmem((kv_heads, length, HEAD_CHANNELS), BF16), vmem((kv_heads, length, HEAD_CHANNELS), BF16),
+        vmem((rows, q_width), F32),
+        vmem((kv_heads // 2, n, rows, 2 * LANES), BF16),
+        vmem((kv_heads // 2, n, rows, 2 * LANES), BF16),
+        vmem((dp, rows, 2 * kv_width), BF16), vmem((dp, share, rows), BF16),
+        vmem((n, share // n, 2 * kv_width), BF16), vmem((n, share // n, 2 * kv_width), BF16),
+        vmem((n, share // n, 2 * kv_width), BF16),
+        dma((9,)), dma((2, n)), dma((2, n)), dma((dp,)), dma((dp,)),
+        dma((2, dp)), dma((2, dp)), dma((2, dp)),
+        dma((kv_heads // 2, n)), dma((kv_heads // 2, n)),
+        dma((dp,)), dma((dp,)), dma((dp,)), dma((n,)), dma((n,)), dma((n,)), dma((n,)),
+    ]
+    hbm = pl.BlockSpec(memory_space=pl.ANY)
+    here = pl.BlockSpec(memory_space=pltpu.VMEM)
+    dx, dq, kw, vw = pl.pallas_call(
+        functools.partial(step_kernel, n, dp),
+        out_shape=(
+            jax.ShapeDtypeStruct((rows, width), BF16),
+            jax.ShapeDtypeStruct((rows, q_width), BF16),
+            jax.ShapeDtypeStruct((share, kv_width), F32),
+            jax.ShapeDtypeStruct((share, kv_width), F32),
+        ),
+        in_specs=[hbm] * 5 + [here] * 2 + [hbm] * 4,
+        out_specs=[here] * 4,
+        scratch_shapes=scratch,
+        compiler_params=pltpu.CompilerParams(
+            collective_id=0, has_side_effects=True, vmem_limit_bytes=56 * 1024 * 1024
+        ),
+    )(
+        inputs[0], queries[0], keys[0], values[0], out_grad[0],
+        jnp.tile(query_gain, 2)[None], jnp.tile(key_gain, 2)[None],
+        key_matrix, value_matrix, jnp.asarray(cos_tab), jnp.asarray(sin_tab),
+    )
+    return dx[None], dq[None], kw, vw
+
+
+def device_step(inputs, *rest):
+    n = lax.axis_size("sp")
+    dp = lax.axis_size("dp")
+    rows, width = inputs.shape[1:]
+    fits = dp % 2 == 0 and width % (dp * LANES) == 0 and rows % LANES == 0 and rows * n <= 1024
+    if fits and (width // dp) % (16 * n) == 0:
+        return kernel_step(n, dp, inputs, *rest)
+    return on_device(inputs, *rest)
+
+
 def solution(mesh):
     return jax.shard_map(
-        on_device,
+        device_step,
         mesh=mesh,
         in_specs=(
             P("dp", "sp", None),

time: 185 us -> 65.3 us (0.35)
  Pallas kernels: 0 us -> 57.8 us
  waiting for transfers between devices: 49.9 us -> 0 us
  blocking collectives: 44.5 us -> 0 us
  starting transfers between devices: 29.8 us -> 0 us
  local copies, waits for them, and re-layouts: 20.9 us -> 6.62 us
  between operations: 14.5 us -> 0.66 us
  matrix products: 12.8 us -> 0 us
  other arithmetic: 11.5 us -> 0 us
    pallas_call x0 -> x1, Pallas kernels: none -> 57.8 us  [kernel_step(): pl.pallas_call(functools.partial(step_kernel, n, dp), out_shape=(jax.Shap...]
    all_gather x2 -> x0, blocking collectives: 34.2 us -> none  [the longest x1 19 us: on_device(): all_grads = lax.all_gather(projection_gradient, 'sp', axis=0, tiled=True)]
    all_to_all x7 -> x0, starting transfers between devices: 29.5 us -> none  [the longest x1 6.35 us: on_device(): lax.all_to_all(key_positions, 'sp', split_axis=1, concat_axis=0, tiled=True)]
    all_to_all x7 -> x0, waiting for transfers between devices: 21.9 us -> none  [the longest x1 5.66 us: on_device(): lax.all_to_all(out_grad[0], 'sp', split_axis=1, concat_axis=0, tiled=True)]
    reduce_scatter x1 -> x0, waiting for transfers between devices: 15.1 us -> none  [on_device(): lax.psum_scatter(lax.dot_general(share_cols, all_grads, (((0,), (0,)), ((...]
    all_gather x1 -> x0, waiting for transfers between devices: 12.8 us -> none  [on_device(): lax.all_gather(joined_weight, 'dp', axis=0, tiled=True)]
    dot_general x7 -> x0, matrix products: 12.8 us -> none  [the longest x5 7.27 us: product(): jnp.einsum(pattern, first_op, second_op, preferred_element_type=jnp.float32)]
    all_to_all x1 -> x0, blocking collectives: 10.3 us -> none  [on_device(): lax.all_to_all(query_part.reshape(token_length, local_heads * HEAD_CHANNE...]
  transfers between devices with their start and end apart: 9 -> 0, of which waited for: 8 -> 0; matrix products, arithmetic and copies ran while one was open for 14% -> 0% of each run, Pallas kernels for 0% -> 0%
where the time goes in v1:
time: 65.3 us; the launch traced here: 65 us
  Pallas kernels  57.8 us (89%)
  local copies, waits for them, and re-layouts  6.62 us (10%)
  between operations  0.66 us (1%)
    pallas_call x1, Pallas kernels, kernel_step(): pl.pallas_call(functools.partial(step_kernel, n, dp), out_shape=(jax.Shap...  57.8 us
    unnamed x14, local copies, waits for them, and re-layouts  5.43 us

profile of v1, /device:TPU:0, one launch (start us, length us, event | category | flops | bytes accessed | tf_op | source)
XLA Modules:
  0.0 65.0 jit_solution(5483025839105235916)
XLA Ops:
  0.6 0.0 copy-start.3
  0.6 0.6 copy-done.3
  1.3 0.0 copy-start.4
  1.3 0.6 broadcast_in_dim_tile.6.qg_ref
  1.9 0.1 copy-done.4
  1.9 0.6 broadcast_in_dim_tile.7.kg_ref
  2.5 57.8 %shard_map.138 = (bf16[128,2048]{1,0:T(8,128)(2,1)}, bf16[128,1024]{1,0:T(8,128)(2,1)}, f32[256,256]{1,0:T(8,128)}, f32[256,256]{1,0:T(8,128)}) custom-call(bf16[128,2048]{1,0:T(8,128)(2,1)} %bitcast.7, bf16[128,1024]{1,0:T(8,128)(2,1)} %bitcast.9, bf16[128,256]{1,0:T(8,128)(2,1)} %bitcast.12, bf16[128,256]{1,0:T(8,128)(2,1)} %bitcast.13, ...), custom_call_target="tpu_custom_call" | custom-call | tf_op jit(solution)/shard_map/pallas_call | solution.py:554
  60.3 0.0 copy-start.2
  60.3 1.9 %copy.19 = bf16[1,128,2048]{2,1,0:T(8,128)(2,1)} copy(bf16[1,128,2048]{2,1,0:T(8,128)(2,1)} %bitcast.8) | data formatting | bytes 1048576
  62.2 0.0 copy-done.2
  62.2 0.0 copy-start.1
  62.2 0.7 %copy.20 = bf16[1,128,1024]{2,1,0:T(8,128)(2,1)} copy(bf16[1,128,1024]{2,1,0:T(8,128)(2,1)S(1)} %bitcast.11) | data formatting | bytes 524288
  62.9 0.3 copy-done.1
  63.3 0.0 copy-start
  63.3 0.7 %copy.21 = f32[256,256]{1,0:T(8,128)} copy(f32[256,256]{1,0:T(8,128)S(1)} %copy-done.1) | data formatting | bytes 524288
  64.0 0.3 copy-done
  64.3 0.7 %copy.22 = f32[256,256]{1,0:T(8,128)} copy(f32[256,256]{1,0:T(8,128)S(1)} %copy-done) | data formatting | bytes 524288
  (2 shorter events, 0.0 us)
Async XLA Ops:
  0.6 0.7 %copy-start.3 = (f32[64]{0:T(128)S(1)}, f32[64]{0:T(128)}, u32[]{:S(2)}) copy-start(f32[64]{0:T(128)} %param.16) | copy-start | bytes 772
  1.3 0.7 %copy-start.4 = (f32[64]{0:T(128)S(1)}, f32[64]{0:T(128)}, u32[]{:S(2)}) copy-start(f32[64]{0:T(128)} %param.17) | copy-start | bytes 772
  60.3 1.9 %copy-start.2 = (bf16[128,1024]{1,0:T(8,128)(2,1)S(1)}, bf16[128,1024]{1,0:T(8,128)(2,1)}, u32[]{:S(2)}) copy-start(bf16[128,1024]{1,0:T(8,128)(2,1)} %get-tuple-element.9) | copy-start | bytes 786436
  62.2 1.0 %copy-start.1 = (f32[256,256]{1,0:T(8,128)S(1)}, f32[256,256]{1,0:T(8,128)}, u32[]{:S(2)}) copy-start(f32[256,256]{1,0:T(8,128)} %get-tuple-element.18) | copy-start | bytes 786436
  63.3 1.0 %copy-start = (f32[256,256]{1,0:T(8,128)S(1)}, f32[256,256]{1,0:T(8,128)}, u32[]{:S(2)}) copy-start(f32[256,256]{1,0:T(8,128)} %get-tuple-element.19) | copy-start | bytes 786436

commit v2 on v1

--- a/solution.py
+++ b/solution.py
@@ -281,21 +281,21 @@
 def step_kernel(
     n, dp,
     x_hbm, q_hbm, k_hbm, v_hbm, do_hbm, qg_ref, kg_ref, km_hbm, vm_hbm, cos_hbm, sin_hbm,
-    dx_ref, dq_ref, kw_ref, vw_ref,
+    dx_out, dq_out, fin_out,
     q_buf, do_buf, cos_buf, sin_buf, k_all, v_all, x_all, wk_all, wv_all,
-    q_st, do_st, k_st, v_st, dq_acc, part, got, g_all, x_t, wg_part, wg_got, fin_all,
-    local_sem, kv_send, kv_recv, x_send, x_recv, w_send, w_recv, w_fsend,
+    q_st, do_st, k_st, v_st, dq_acc, dq_buf, dx_buf, part, got, g_all, x_t, wg_part, wg_got,
+    fin_all,
+    local_sem, out_sem, kv_send, kv_recv, x_send, x_recv, w_send, w_recv, w_fsend,
     p_send, p_recv, g_send, g_recv, g_fsend, r_send, r_recv, f_send, f_recv,
 ):
     me = lax.axis_index("sp")
     md = lax.axis_index("dp")
     rows, q_width = q_buf.shape
-    kv_width = k_all.shape[2]
+    head_pairs = k_all.shape[0]
     share = x_all.shape[2]
-    kv_heads = kv_width // HEAD_CHANNELS
-    per_group = q_width // kv_width
+    per_group = q_width // (2 * head_pairs * HEAD_CHANNELS)
     mate = md + 1 - 2 * (md % 2)
-    pairs = dp // 2
+    piece = share // n
 
     def sp_peer(o):
         return lax.rem(me + o, n)
@@ -308,6 +308,12 @@
 
     def dp_from(o):
         return lax.rem(md - o + dp, dp)
+
+    def mate_from(o):
+        return lax.rem(mate - o + dp, dp)
+
+    def pair(c):
+        return pl.ds(c * LANES, LANES)
 
     barrier = pltpu.get_barrier_semaphore()
     for o in range(1, n):
@@ -318,14 +324,16 @@
     def columns(d):
         return pl.ds(pl.multiple_of(d * share, share), share)
 
+    wanted = [
+        (q_hbm, q_buf), (do_hbm, do_buf), (cos_hbm, cos_buf), (sin_hbm, sin_buf),
+        (x_hbm.at[:, columns(md)], x_all.at[md]),
+        (km_hbm, wk_all.at[md]), (vm_hbm, wv_all.at[md]),
+    ]
+    for c in range(head_pairs):
+        wanted.append((k_hbm.at[:, pair(c)], k_all.at[c, me]))
+        wanted.append((v_hbm.at[:, pair(c)], v_all.at[c, me]))
     local = [
-        pltpu.make_async_copy(src, dst, local_sem.at[i])
-        for i, (src, dst) in enumerate([
-            (q_hbm, q_buf), (do_hbm, do_buf), (cos_hbm, cos_buf), (sin_hbm, sin_buf),
-            (k_hbm, k_all.at[me]), (v_hbm, v_all.at[me]),
-            (x_hbm.at[:, columns(md)], x_all.at[md]),
-            (km_hbm, wk_all.at[md]), (vm_hbm, wv_all.at[md]),
-        ])
+        pltpu.make_async_copy(src, dst, local_sem.at[i]) for i, (src, dst) in enumerate(wanted)
     ]
     for copy in local:
         copy.start()
@@ -349,9 +357,11 @@
         remote(dst, dst, recv, recv, {"sp": me}).wait_recv()
 
     order = sorted(range(1, n), key=lambda o: -min(o, n - o))
-    for kind, (src, dst) in enumerate([(k_hbm, k_all), (v_hbm, v_all)]):
-        for o in order:
-            send(src, dst.at[me], kv_send.at[kind, o], kv_recv.at[kind, me], {"sp": sp_peer(o)})
+    for c in range(head_pairs):
+        for kind, (src, dst) in enumerate([(k_hbm, k_all), (v_hbm, v_all)]):
+            for o in order:
+                send(src.at[:, pair(c)], dst.at[c, me], kv_send.at[kind, c, o],
+                     kv_recv.at[kind, c, me], {"sp": sp_peer(o)})
     weights = [(km_hbm, wk_all), (vm_hbm, wv_all)]
     for kind, (src, dst) in enumerate(weights):
         for o in range(2, dp, 2):
@@ -367,13 +377,12 @@
     my_rows = pl.ds(pl.multiple_of(me * rows, rows), rows)
     cos_own = cos_buf[my_rows, :]
     sin_own = sin_buf[my_rows, :]
-    q_gain = qg_ref[...]
-    k_gain = kg_ref[...]
+    q_gain = jnp.concatenate([qg_ref[...], qg_ref[...]], axis=1)
+    k_gain = jnp.concatenate([kg_ref[...], kg_ref[...]], axis=1)
 
     for c in range(q_width // LANES):
-        lanes = pl.ds(c * LANES, LANES)
-        turned = norm_rotate(q_buf[:, lanes].astype(F32), q_gain, cos_own, sin_own).astype(BF16)
-        grads = do_buf[:, lanes]
+        turned = norm_rotate(q_buf[:, pair(c)].astype(F32), q_gain, cos_own, sin_own).astype(BF16)
+        grads = do_buf[:, pair(c)]
         for a in range(2):
             h = 2 * c + a
             to = pl.ds((h % per_group) * rows, rows)
@@ -381,25 +390,16 @@
             q_st[h // per_group, to, :] = turned[:, half]
             do_st[h // per_group, to, :] = grads[:, half]
 
-    def stack_keys(src):
+    def stack_keys(c, src):
         at = pl.ds(pl.multiple_of(src * rows, rows), rows)
-        for c in range(kv_width // LANES):
-            lanes = pl.ds(c * LANES, LANES)
-            turned = norm_rotate(
-                k_all[src, :, lanes].astype(F32), k_gain, cos_buf[at, :], sin_buf[at, :]
-            ).astype(BF16)
-            vals = v_all[src, :, lanes]
-            for a in range(2):
-                half = slice(a * HEAD_CHANNELS, (a + 1) * HEAD_CHANNELS)
-                k_st[2 * c + a, at, :] = turned[:, half]
-                v_st[2 * c + a, at, :] = vals[:, half]
-
-    stack_keys(me)
-    for o in range(1, n):
-        src = sp_from(o)
-        arrived(k_all.at[src], kv_recv.at[0, src])
-        arrived(v_all.at[src], kv_recv.at[1, src])
-        stack_keys(src)
+        turned = norm_rotate(
+            k_all[c, src].astype(F32), k_gain, cos_buf[at, :], sin_buf[at, :]
+        ).astype(BF16)
+        vals = v_all[c, src]
+        for a in range(2):
+            half = slice(a * HEAD_CHANNELS, (a + 1) * HEAD_CHANNELS)
+            k_st[2 * c + a, at, :] = turned[:, half]
+            v_st[2 * c + a, at, :] = vals[:, half]
 
     def attend(g):
         qs = q_st[g]
@@ -423,7 +423,14 @@
             dq_acc[:, head * HEAD_CHANNELS:head * HEAD_CHANNELS + LANES] = both.T
         return key_part, value_part
 
-    for c in range(kv_heads // 2):
+    for c in range(head_pairs):
+        stack_keys(c, me)
+    for c in range(head_pairs):
+        for o in range(1, n):
+            src = sp_from(o)
+            arrived(k_all.at[c, src], kv_recv.at[0, c, src])
+            arrived(v_all.at[c, src], kv_recv.at[1, c, src])
+            stack_keys(c, src)
         key_low, value_low = attend(2 * c)
         key_high, value_high = attend(2 * c + 1)
         both = jnp.concatenate([key_low, key_high, value_low, value_high], axis=1).astype(BF16)
@@ -433,17 +440,53 @@
             send(part.at[c, sp_peer(o)], got.at[c, me], p_send.at[c, o], p_recv.at[c, me],
                  {"sp": sp_peer(o)})
 
-    for kind, (_, dst) in enumerate(weights):
+    def own_grads(c):
+        total = part[c, me].astype(F32)
+        for o in range(1, n):
+            src = sp_from(o)
+            arrived(got.at[c, src], p_recv.at[c, src])
+            total = total + got[c, src].astype(F32)
+        g_all[c, md, :, :LANES] = norm_rotate_back(
+            k_all[c, me].astype(F32), total[:, :LANES], k_gain, cos_own, sin_own
+        ).astype(BF16)
+        g_all[c, md, :, LANES:] = total[:, LANES:].astype(BF16)
+        mine = g_all.at[c, md]
+        for o in range(2, dp, 2):
+            send(mine, mine, g_send.at[c, o], g_recv.at[c, md], {"dp": dp_peer(o)})
+        send(mine, mine, g_send.at[c, 1], g_recv.at[c, md], {"dp": mate})
+
+    def pass_on(c):
         for o in range(2, dp, 2):
             src = dp_from(o)
-            arrived(dst.at[src], w_recv.at[kind, src])
-            send(dst.at[src], dst.at[src], w_fsend.at[kind, o], w_recv.at[kind, src], {"dp": mate})
-
-    for c in range(q_width // LANES):
-        lanes = pl.ds(c * LANES, LANES)
-        dq_ref[:, lanes] = norm_rotate_back(
-            q_buf[:, lanes].astype(F32), dq_acc[:, lanes], q_gain, cos_own, sin_own
-        ).astype(BF16)
+            theirs = g_all.at[c, src]
+            arrived(theirs, g_recv.at[c, src])
+            send(theirs, theirs, g_fsend.at[c, o], g_recv.at[c, src], {"dp": mate})
+
+    def weight_grads(c):
+        total = contract(x_t[md], g_all[c, md], ((1,), (0,)))
+        for o in range(2, dp, 2):
+            src = dp_from(o)
+            total = total + contract(x_t[src], g_all[c, src], ((1,), (0,)))
+        for o in range(0, dp, 2):
+            src = mate_from(o)
+            arrived(g_all.at[c, src], g_recv.at[c, src])
+            total = total + contract(x_t[src], g_all[c, src], ((1,), (0,)))
+        for j in range(n):
+            wg_part[c, j] = total[j * piece:(j + 1) * piece, :].astype(BF16)
+        for o in order:
+            send(wg_part.at[c, sp_peer(o)], wg_got.at[c, me], r_send.at[c, o], r_recv.at[c, me],
+                 {"sp": sp_peer(o)})
+
+    def sum_weight_grads(c):
+        total = wg_part[c, me].astype(F32)
+        for o in range(1, n):
+            src = sp_from(o)
+            arrived(wg_got.at[c, src], r_recv.at[c, src])
+            total = total + wg_got[c, src].astype(F32)
+        fin_all[c, me] = total.astype(BF16)
+        mine = fin_all.at[c, me]
+        for o in order:
+            send(mine, mine, f_send.at[c, o], f_recv.at[c, me], {"sp": sp_peer(o)})
 
     for o in range(dp):
         src = dp_from(o)
@@ -451,70 +494,87 @@
             arrived(x_all.at[src], x_recv.at[src])
         x_t[src] = x_all[src].T
 
-    for c in range(kv_heads // 2):
-        total = part[c, me].astype(F32)
-        for o in range(1, n):
-            src = sp_from(o)
-            arrived(got.at[c, src], p_recv.at[c, src])
-            total = total + got[c, src].astype(F32)
-        lanes = pl.ds(c * LANES, LANES)
-        g_all[md, :, lanes] = norm_rotate_back(
-            k_all[me, :, lanes].astype(F32), total[:, :LANES], k_gain, cos_own, sin_own
-        ).astype(BF16)
-        g_all[md, :, pl.ds(kv_width + c * LANES, LANES)] = total[:, LANES:].astype(BF16)
-    for o in range(2, dp, 2):
-        send(g_all.at[md], g_all.at[md], g_send.at[o], g_recv.at[md], {"dp": dp_peer(o)})
-    send(g_all.at[md], g_all.at[md], g_send.at[1], g_recv.at[md], {"dp": mate})
-
-    own = g_all[md]
-    wgrad = contract(x_t[md], own, ((1,), (0,)))
+    for c in range(head_pairs):
+        own_grads(c)
+        if c == 0:
+            for kind, (_, dst) in enumerate(weights):
+                for o in range(2, dp, 2):
+                    src = dp_from(o)
+                    arrived(dst.at[src], w_recv.at[kind, src])
+                    send(dst.at[src], dst.at[src], w_fsend.at[kind, o], w_recv.at[kind, src],
+                         {"dp": mate})
+            for i in range(q_width // LANES):
+                dq_buf[:, pair(i)] = norm_rotate_back(
+                    q_buf[:, pair(i)].astype(F32), dq_acc[:, pair(i)], q_gain, cos_own, sin_own
+                ).astype(BF16)
+            dq_copy = pltpu.make_async_copy(dq_buf, dq_out, out_sem.at[0])
+            dq_copy.start()
+
+    own = jnp.concatenate(
+        [g_all[c, md, :, :LANES] for c in range(head_pairs)]
+        + [g_all[c, md, :, LANES:] for c in range(head_pairs)], axis=1)
+    kv_width = head_pairs * LANES
 
     def project(src):
         out = contract(own[:, :kv_width], wk_all[src], ((1,), (1,)))
         out = out + contract(own[:, kv_width:], wv_all[src], ((1,), (1,)))
-        dx_ref[:, columns(src)] = out.astype(BF16)
-
-    project(md)
-    for o in range(2, dp, 2):
+        dx_buf[:, columns(src)] = out.astype(BF16)
+
+    for c in range(head_pairs):
+        pass_on(c)
+        weight_grads(c)
+    for o in range(0, dp, 2):
         project(dp_from(o))
-    for o in range(2, dp, 2):
-        src = dp_from(o)
-        arrived(g_all.at[src], g_recv.at[src])
-        send(g_all.at[src], g_all.at[src], g_fsend.at[o], g_recv.at[src], {"dp": mate})
-        wgrad = wgrad + contract(x_t[src], g_all[src], ((1,), (0,)))
     for o in range(0, dp, 2):
-        src = lax.rem(mate - o + dp, dp)
-        arrived(g_all.at[src], g_recv.at[src])
-        wgrad = wgrad + contract(x_t[src], g_all[src], ((1,), (0,)))
-
-    piece = share // n
-    for j in range(n):
-        wg_part[j] = wgrad[j * piece:(j + 1) * piece, :].astype(BF16)
-    for o in order:
-        send(wg_part.at[sp_peer(o)], wg_got.at[me], r_send.at[o], r_recv.at[me],
-             {"sp": sp_peer(o)})
-    for o in range(0, dp, 2):
-        src = lax.rem(mate - o + dp, dp)
+        src = mate_from(o)
         for kind, (_, dst) in enumerate(weights):
             arrived(dst.at[src], w_recv.at[kind, src])
         project(src)
-    total = wg_part[me].astype(F32)
-    for o in range(1, n):
-        src = sp_from(o)
-        arrived(wg_got.at[src], r_recv.at[src])
-        total = total + wg_got[src].astype(F32)
-    fin_all[me] = total.astype(BF16)
-    for o in order:
-        send(fin_all.at[me], fin_all.at[me], f_send.at[o], f_recv.at[me], {"sp": sp_peer(o)})
-    for o in range(n):
-        src = sp_from(o)
-        if o:
-            arrived(fin_all.at[src], f_recv.at[src])
-        at = pl.ds(pl.multiple_of(src * piece, piece), piece)
-        kw_ref[at, :] = fin_all[src, :, :kv_width].astype(F32)
-        vw_ref[at, :] = fin_all[src, :, kv_width:].astype(F32)
+    dx_copy = pltpu.make_async_copy(dx_buf, dx_out, out_sem.at[1])
+    dx_copy.start()
+    for c in range(head_pairs):
+        sum_weight_grads(c)
+    for c in range(head_pairs):
+        for o in range(1, n):
+            src = sp_from(o)
+            arrived(fin_all.at[c, src], f_recv.at[c, src])
+    fin_copy = pltpu.make_async_copy(fin_all, fin_out, out_sem.at[2])
+    fin_copy.start()
     for copy in sends:
         copy.wait_send()
+    dq_copy.wait()
+    dx_copy.wait()
+    fin_copy.wait()
+
+
+def write_kernel(dx_hbm, dq_hbm, fin_hbm, dx_out, dq_out, kw_out, vw_out,
+                 dx_buf, dq_buf, fin_buf, kw_buf, vw_buf, in_sem, out_sem):
+    loads = [
+        pltpu.make_async_copy(src, dst, in_sem.at[i])
+        for i, (src, dst) in enumerate([(fin_hbm, fin_buf), (dx_hbm, dx_buf), (dq_hbm, dq_buf)])
+    ]
+    stores = [
+        pltpu.make_async_copy(src, dst, out_sem.at[i])
+        for i, (src, dst) in enumerate(
+            [(dx_buf, dx_out), (dq_buf, dq_out), (kw_buf, kw_out), (vw_buf, vw_out)])
+    ]
+    for copy in loads:
+        copy.start()
+    head_pairs, n, piece, _ = fin_buf.shape
+    loads[0].wait()
+    for c in range(head_pairs):
+        for j in range(n):
+            at = pl.ds(j * piece, piece)
+            kw_buf[at, pl.ds(c * LANES, LANES)] = fin_buf[c, j, :, :LANES].astype(F32)
+            vw_buf[at, pl.ds(c * LANES, LANES)] = fin_buf[c, j, :, LANES:].astype(F32)
+    stores[2].start()
+    stores[3].start()
+    loads[1].wait()
+    stores[0].start()
+    loads[2].wait()
+    stores[1].start()
+    for copy in stores:
+        copy.wait()
 
 
 def kernel_step(
@@ -526,50 +586,62 @@
     length = rows * n
     share = width // dp
     kv_heads = kv_width // HEAD_CHANNELS
+    half = kv_heads // 2
     stack = rows * (q_width // kv_width)
     cos_tab, sin_tab = pair_tables(length)
-    vmem = functools.partial(pltpu.VMEM)
+    vmem = pltpu.VMEM
     dma = pltpu.SemaphoreType.DMA
+    wide = 2 * LANES
     scratch = [
         vmem((rows, q_width), BF16), vmem((rows, q_width), BF16),
         vmem((length, LANES), F32), vmem((length, LANES), F32),
-        vmem((n, rows, kv_width), BF16), vmem((n, rows, kv_width), BF16),
+        vmem((half, n, rows, LANES), BF16), vmem((half, n, rows, LANES), BF16),
         vmem((dp, rows, share), BF16),
         vmem((dp, share, kv_width), BF16), vmem((dp, share, kv_width), BF16),
         vmem((kv_heads, stack, HEAD_CHANNELS), BF16), vmem((kv_heads, stack, HEAD_CHANNELS), BF16),
         vmem((kv_heads, length, HEAD_CHANNELS), BF16), vmem((kv_heads, length, HEAD_CHANNELS), BF16),
-        vmem((rows, q_width), F32),
-        vmem((kv_heads // 2, n, rows, 2 * LANES), BF16),
-        vmem((kv_heads // 2, n, rows, 2 * LANES), BF16),
-        vmem((dp, rows, 2 * kv_width), BF16), vmem((dp, share, rows), BF16),
-        vmem((n, share // n, 2 * kv_width), BF16), vmem((n, share // n, 2 * kv_width), BF16),
-        vmem((n, share // n, 2 * kv_width), BF16),
-        dma((9,)), dma((2, n)), dma((2, n)), dma((dp,)), dma((dp,)),
+        vmem((rows, q_width), F32), vmem((rows, q_width), BF16), vmem((rows, width), BF16),
+        vmem((half, n, rows, wide), BF16), vmem((half, n, rows, wide), BF16),
+        vmem((half, dp, rows, wide), BF16), vmem((dp, share, rows), BF16),
+        vmem((half, n, share // n, wide), BF16), vmem((half, n, share // n, wide), BF16),
+        vmem((half, n, share // n, wide), BF16),
+        dma((7 + 2 * half,)), dma((3,)),
+        dma((2, half, n)), dma((2, half, n)), dma((dp,)), dma((dp,)),
         dma((2, dp)), dma((2, dp)), dma((2, dp)),
-        dma((kv_heads // 2, n)), dma((kv_heads // 2, n)),
-        dma((dp,)), dma((dp,)), dma((dp,)), dma((n,)), dma((n,)), dma((n,)), dma((n,)),
+        dma((half, n)), dma((half, n)),
+        dma((half, dp)), dma((half, dp)), dma((half, dp)),
+        dma((half, n)), dma((half, n)), dma((half, n)), dma((half, n)),
     ]
     hbm = pl.BlockSpec(memory_space=pl.ANY)
     here = pl.BlockSpec(memory_space=pltpu.VMEM)
-    dx, dq, kw, vw = pl.pallas_call(
+    dx_type = jax.ShapeDtypeStruct((rows, width), BF16)
+    dq_type = jax.ShapeDtypeStruct((rows, q_width), BF16)
+    kw_type = jax.ShapeDtypeStruct((share, kv_width), F32)
+    fin_shape = (half, n, share // n, wide)
+    dx, dq, fin = pl.pallas_call(
         functools.partial(step_kernel, n, dp),
-        out_shape=(
-            jax.ShapeDtypeStruct((rows, width), BF16),
-            jax.ShapeDtypeStruct((rows, q_width), BF16),
-            jax.ShapeDtypeStruct((share, kv_width), F32),
-            jax.ShapeDtypeStruct((share, kv_width), F32),
-        ),
+        out_shape=(dx_type, dq_type, jax.ShapeDtypeStruct(fin_shape, BF16)),
         in_specs=[hbm] * 5 + [here] * 2 + [hbm] * 4,
-        out_specs=[here] * 4,
+        out_specs=[hbm] * 3,
         scratch_shapes=scratch,
         compiler_params=pltpu.CompilerParams(
             collective_id=0, has_side_effects=True, vmem_limit_bytes=56 * 1024 * 1024
         ),
     )(
         inputs[0], queries[0], keys[0], values[0], out_grad[0],
-        jnp.tile(query_gain, 2)[None], jnp.tile(key_gain, 2)[None],
+        query_gain[None], key_gain[None],
         key_matrix, value_matrix, jnp.asarray(cos_tab), jnp.asarray(sin_tab),
     )
+    dx, dq, kw, vw = pl.pallas_call(
+        write_kernel,
+        out_shape=(dx_type, dq_type, kw_type, kw_type),
+        in_specs=[hbm] * 3,
+        out_specs=[hbm] * 4,
+        scratch_shapes=[
+            vmem((rows, width), BF16), vmem((rows, q_width), BF16), vmem(fin_shape, BF16),
+            vmem((share, kv_width), F32), vmem((share, kv_width), F32), dma((3,)), dma((4,)),
+        ],
+    )(dx, dq, fin)
     return dx[None], dq[None], kw, vw
 
 

time: 65.3 us -> 52 us (0.80)
  Pallas kernels: 57.8 us -> 50.7 us
  local copies, waits for them, and re-layouts: 6.62 us -> 0 us
    pallas_call x1 -> x2, Pallas kernels: 57.8 us -> 50.7 us  [the longest x1 48.6 us: kernel_step(): pl.pallas_call(functools.partial(step_kernel, n, dp), out_shape=(dx_type,...]
    unnamed x14 -> x0, local copies, waits for them, and re-layouts: 5.43 us -> none
    another operation x4 -> x0, local copies, waits for them, and re-layouts: 1.19 us -> none  [the longest x2 0.59 us: kernel_step(): jnp.tile(key_gain, 2)[None]]
where the time goes in v2:
time: 52 us; the launch traced here: 51.3 us
  Pallas kernels  50.7 us (98%)
  between operations  0.64 us (1%)
    pallas_call x1, Pallas kernels, kernel_step(): pl.pallas_call(functools.partial(step_kernel, n, dp), out_shape=(dx_type,...  48.6 us
    pallas_call x1, Pallas kernels, kernel_step(): pl.pallas_call(write_kernel, out_shape=(dx_type, dq_type, kw_type, kw_typ...  2.09 us

profile of v2, /device:TPU:0, one launch (start us, length us, event | category | flops | bytes accessed | tf_op | source)
XLA Modules:
  0.0 51.3 jit_solution(7243211108105708823)
XLA Ops:
  0.6 48.6 %shard_map.138 = (bf16[128,2048]{1,0:T(8,128)(2,1)}, bf16[128,1024]{1,0:T(8,128)(2,1)}, bf16[2,4,64,256]{3,2,1,0:T(8,128)(2,1)}) custom-call(bf16[128,2048]{1,0:T(8,128)(2,1)} %bitcast.9, bf16[128,1024]{1,0:T(8,128)(2,1)} %bitcast.10, bf16[128,256]{1,0:T(8,128)(2,1)} %bitcast.12, bf16[128,256]{1,0:T(8,128)(2,1)} %bitcast.13, bf16[128,1024]{1,0:T(8,128)(2,1)} %bitcast.11, ...), custom_call_target="tpu_custom_call" | custom-call | tf_op jit(solution)/shard_map/pallas_call | solution.py:621
  49.2 2.1 %shard_map.139 = (bf16[128,2048]{1,0:T(8,128)(2,1)}, bf16[128,1024]{1,0:T(8,128)(2,1)}, f32[256,256]{1,0:T(8,128)}, f32[256,256]{1,0:T(8,128)}) custom-call(bf16[128,2048]{1,0:T(8,128)(2,1)} %get-tuple-element.11.dx_hbm, bf16[128,1024]{1,0:T(8,128)(2,1)} %get-tuple-element.12.dq_hbm, bf16[2,4,64,256]{3,2,1,0:T(8,128)(2,1)} %get-tuple-element.13.fin_hbm), custom_call_target="tpu_custom_call" | custom-call | tf_op jit(solution)/shard_map/pallas_call | solution.py:635

commit v3 on v2

--- a/solution.py
+++ b/solution.py
@@ -224,6 +224,7 @@
 
 
 LANES = 128
+VMEM_BYTES = 67043328
 MESH = pl.DeviceIdType.MESH
 F32 = jnp.float32
 BF16 = jnp.bfloat16
@@ -280,13 +281,13 @@
 
 def step_kernel(
     n, dp,
-    x_hbm, q_hbm, k_hbm, v_hbm, do_hbm, qg_ref, kg_ref, km_hbm, vm_hbm, cos_hbm, sin_hbm,
-    dx_out, dq_out, fin_out,
-    q_buf, do_buf, cos_buf, sin_buf, k_all, v_all, x_all, wk_all, wv_all,
-    q_st, do_st, k_st, v_st, dq_acc, dq_buf, dx_buf, part, got, g_all, x_t, wg_part, wg_got,
+    x_hbm, q_hbm, k_hbm, v_hbm, do_hbm, qg_hbm, kg_hbm, km_hbm, vm_hbm, cos_hbm, sin_hbm,
+    dx_buf, dq_buf, kw_buf, vw_buf,
+    qg_ref, kg_ref, q_buf, do_buf, cos_buf, sin_buf, k_all, v_all, x_all, wk_all, wv_all,
+    q_st, do_st, k_st, v_st, dq_acc, part, got, far, g_all, x_t, wg_part, wg_got,
     fin_all,
-    local_sem, out_sem, kv_send, kv_recv, x_send, x_recv, w_send, w_recv, w_fsend,
-    p_send, p_recv, g_send, g_recv, g_fsend, r_send, r_recv, f_send, f_recv,
+    local_sem, kv_send, kv_recv, x_send, x_recv, w_send, w_recv, w_fsend,
+    kv_fsend, far_send, far_recv, p_send, p_recv, g_send, g_recv, g_fsend, r_send, r_recv, f_send, f_recv,
 ):
     me = lax.axis_index("sp")
     md = lax.axis_index("dp")
@@ -327,7 +328,7 @@
     wanted = [
         (q_hbm, q_buf), (do_hbm, do_buf), (cos_hbm, cos_buf), (sin_hbm, sin_buf),
         (x_hbm.at[:, columns(md)], x_all.at[md]),
-        (km_hbm, wk_all.at[md]), (vm_hbm, wv_all.at[md]),
+        (km_hbm, wk_all.at[md]), (vm_hbm, wv_all.at[md]), (qg_hbm, qg_ref), (kg_hbm, kg_ref),
     ]
     for c in range(head_pairs):
         wanted.append((k_hbm.at[:, pair(c)], k_all.at[c, me]))
@@ -348,20 +349,32 @@
 
     sends = []
 
-    def send(*args):
+    def only_if(condition, act):
+        if condition is None:
+            act()
+        else:
+            pl.when(condition)(act)
+
+    def send(*args, condition=None):
         copy = remote(*args)
-        copy.start()
-        sends.append(copy)
+        only_if(condition, copy.start)
+        sends.append((condition, copy))
 
     def arrived(dst, recv):
         remote(dst, dst, recv, recv, {"sp": me}).wait_recv()
 
+    line = n == 4
+    near_right = {1: me != n - 1, n - 1: me != 0} if line else {}
+    near_left = {1: me != 0, n - 1: me != n - 1} if line else {}
+    inner = (me != 0) & (me != n - 1)
+    outer = (me == 0) | (me == n - 1)
+    inward = jnp.where(me == 0, 1, n - 2)
     order = sorted(range(1, n), key=lambda o: -min(o, n - o))
     for c in range(head_pairs):
         for kind, (src, dst) in enumerate([(k_hbm, k_all), (v_hbm, v_all)]):
             for o in order:
                 send(src.at[:, pair(c)], dst.at[c, me], kv_send.at[kind, c, o],
-                     kv_recv.at[kind, c, me], {"sp": sp_peer(o)})
+                     kv_recv.at[kind, c, me], {"sp": sp_peer(o)}, condition=near_right.get(o))
     weights = [(km_hbm, wk_all), (vm_hbm, wv_all)]
     for kind, (src, dst) in enumerate(weights):
         for o in range(2, dp, 2):
@@ -423,28 +436,59 @@
             dq_acc[:, head * HEAD_CHANNELS:head * HEAD_CHANNELS + LANES] = both.T
         return key_part, value_part
 
+    def add_far(c):
+        if not line:
+            return
+        across = sp_peer(2)
+        copy = remote(part.at[c, across], got.at[c, me], p_send.at[c, 2], p_recv.at[c, me],
+                      {"sp": across})
+
+        @pl.when(inner)
+        def _():
+            arrived(far.at[c], far_recv.at[c])
+            part[c, across] = (part[c, across].astype(F32) + far[c].astype(F32)).astype(BF16)
+            copy.start()
+
+        sends.append((inner, copy))
+
+    if line:
+        @pl.when(outer)
+        def _():
+            for c in range(head_pairs):
+                got[c, n - 1 - me] = jnp.zeros(got.shape[2:], BF16)
+
     for c in range(head_pairs):
         stack_keys(c, me)
     for c in range(head_pairs):
-        for o in range(1, n):
+        for o in order:
             src = sp_from(o)
-            arrived(k_all.at[c, src], kv_recv.at[0, c, src])
-            arrived(v_all.at[c, src], kv_recv.at[1, c, src])
+            for kind, ref in enumerate([k_all, v_all]):
+                arrived(ref.at[c, src], kv_recv.at[kind, c, src])
+                if line and o == 2:
+                    send(ref.at[c, src], ref.at[c, src], kv_fsend.at[kind, c],
+                         kv_recv.at[kind, c, src], {"sp": jnp.where(me == 1, 0, n - 1)},
+                         condition=inner)
             stack_keys(c, src)
+        if c:
+            add_far(c - 1)
         key_low, value_low = attend(2 * c)
         key_high, value_high = attend(2 * c + 1)
         both = jnp.concatenate([key_low, key_high, value_low, value_high], axis=1).astype(BF16)
         for j in range(n):
             part[c, j] = both[j * rows:(j + 1) * rows, :]
+        if line:
+            send(part.at[c, n - 1 - me], far.at[c], far_send.at[c], far_recv.at[c],
+                 {"sp": inward}, condition=outer)
         for o in order:
             send(part.at[c, sp_peer(o)], got.at[c, me], p_send.at[c, o], p_recv.at[c, me],
-                 {"sp": sp_peer(o)})
+                 {"sp": sp_peer(o)}, condition=outer if line and o == 2 else near_right.get(o))
+    add_far(head_pairs - 1)
 
     def own_grads(c):
         total = part[c, me].astype(F32)
         for o in range(1, n):
             src = sp_from(o)
-            arrived(got.at[c, src], p_recv.at[c, src])
+            only_if(near_left.get(o), functools.partial(arrived, got.at[c, src], p_recv.at[c, src]))
             total = total + got[c, src].astype(F32)
         g_all[c, md, :, :LANES] = norm_rotate_back(
             k_all[c, me].astype(F32), total[:, :LANES], k_gain, cos_own, sin_own
@@ -507,8 +551,6 @@
                 dq_buf[:, pair(i)] = norm_rotate_back(
                     q_buf[:, pair(i)].astype(F32), dq_acc[:, pair(i)], q_gain, cos_own, sin_own
                 ).astype(BF16)
-            dq_copy = pltpu.make_async_copy(dq_buf, dq_out, out_sem.at[0])
-            dq_copy.start()
 
     own = jnp.concatenate(
         [g_all[c, md, :, :LANES] for c in range(head_pairs)]
@@ -530,50 +572,28 @@
         for kind, (_, dst) in enumerate(weights):
             arrived(dst.at[src], w_recv.at[kind, src])
         project(src)
-    dx_copy = pltpu.make_async_copy(dx_buf, dx_out, out_sem.at[1])
-    dx_copy.start()
     for c in range(head_pairs):
         sum_weight_grads(c)
     for c in range(head_pairs):
-        for o in range(1, n):
+        for o in range(n):
             src = sp_from(o)
-            arrived(fin_all.at[c, src], f_recv.at[c, src])
-    fin_copy = pltpu.make_async_copy(fin_all, fin_out, out_sem.at[2])
-    fin_copy.start()
-    for copy in sends:
-        copy.wait_send()
-    dq_copy.wait()
-    dx_copy.wait()
-    fin_copy.wait()
-
-
-def write_kernel(dx_hbm, dq_hbm, fin_hbm, dx_out, dq_out, kw_out, vw_out,
-                 dx_buf, dq_buf, fin_buf, kw_buf, vw_buf, in_sem, out_sem):
-    loads = [
-        pltpu.make_async_copy(src, dst, in_sem.at[i])
-        for i, (src, dst) in enumerate([(fin_hbm, fin_buf), (dx_hbm, dx_buf), (dq_hbm, dq_buf)])
+            if o:
+                arrived(fin_all.at[c, src], f_recv.at[c, src])
+            at = pl.ds(pl.multiple_of(src * piece, piece), piece)
+            kw_buf[at, pair(c)] = fin_all[c, src, :, :LANES].astype(F32)
+            vw_buf[at, pair(c)] = fin_all[c, src, :, LANES:].astype(F32)
+    for condition, copy in sends:
+        only_if(condition, copy.wait_send)
+
+
+def write_kernel(*refs):
+    count = (len(refs) - 1) // 2
+    copies = [
+        pltpu.make_async_copy(refs[i], refs[count + i], refs[-1].at[i]) for i in range(count)
     ]
-    stores = [
-        pltpu.make_async_copy(src, dst, out_sem.at[i])
-        for i, (src, dst) in enumerate(
-            [(dx_buf, dx_out), (dq_buf, dq_out), (kw_buf, kw_out), (vw_buf, vw_out)])
-    ]
-    for copy in loads:
+    for copy in copies:
         copy.start()
-    head_pairs, n, piece, _ = fin_buf.shape
-    loads[0].wait()
-    for c in range(head_pairs):
-        for j in range(n):
-            at = pl.ds(j * piece, piece)
-            kw_buf[at, pl.ds(c * LANES, LANES)] = fin_buf[c, j, :, :LANES].astype(F32)
-            vw_buf[at, pl.ds(c * LANES, LANES)] = fin_buf[c, j, :, LANES:].astype(F32)
-    stores[2].start()
-    stores[3].start()
-    loads[1].wait()
-    stores[0].start()
-    loads[2].wait()
-    stores[1].start()
-    for copy in stores:
+    for copy in copies:
         copy.wait()
 
 
@@ -593,6 +613,7 @@
     dma = pltpu.SemaphoreType.DMA
     wide = 2 * LANES
     scratch = [
+        vmem((1, HEAD_CHANNELS), F32), vmem((1, HEAD_CHANNELS), F32),
         vmem((rows, q_width), BF16), vmem((rows, q_width), BF16),
         vmem((length, LANES), F32), vmem((length, LANES), F32),
         vmem((half, n, rows, LANES), BF16), vmem((half, n, rows, LANES), BF16),
@@ -600,32 +621,35 @@
         vmem((dp, share, kv_width), BF16), vmem((dp, share, kv_width), BF16),
         vmem((kv_heads, stack, HEAD_CHANNELS), BF16), vmem((kv_heads, stack, HEAD_CHANNELS), BF16),
         vmem((kv_heads, length, HEAD_CHANNELS), BF16), vmem((kv_heads, length, HEAD_CHANNELS), BF16),
-        vmem((rows, q_width), F32), vmem((rows, q_width), BF16), vmem((rows, width), BF16),
+        vmem((rows, q_width), F32),
         vmem((half, n, rows, wide), BF16), vmem((half, n, rows, wide), BF16),
+        vmem((half, rows, wide), BF16),
         vmem((half, dp, rows, wide), BF16), vmem((dp, share, rows), BF16),
         vmem((half, n, share // n, wide), BF16), vmem((half, n, share // n, wide), BF16),
         vmem((half, n, share // n, wide), BF16),
-        dma((7 + 2 * half,)), dma((3,)),
+        dma((9 + 2 * half,)),
         dma((2, half, n)), dma((2, half, n)), dma((dp,)), dma((dp,)),
         dma((2, dp)), dma((2, dp)), dma((2, dp)),
+        dma((2, half)), dma((half,)), dma((half,)),
         dma((half, n)), dma((half, n)),
         dma((half, dp)), dma((half, dp)), dma((half, dp)),
         dma((half, n)), dma((half, n)), dma((half, n)), dma((half, n)),
     ]
-    hbm = pl.BlockSpec(memory_space=pl.ANY)
+    hbm = pl.BlockSpec(memory_space=pltpu.HBM)
     here = pl.BlockSpec(memory_space=pltpu.VMEM)
-    dx_type = jax.ShapeDtypeStruct((rows, width), BF16)
-    dq_type = jax.ShapeDtypeStruct((rows, q_width), BF16)
-    kw_type = jax.ShapeDtypeStruct((share, kv_width), F32)
-    fin_shape = (half, n, share // n, wide)
-    dx, dq, fin = pl.pallas_call(
+    results = [
+        ((rows, width), BF16), ((rows, q_width), BF16),
+        ((share, kv_width), F32), ((share, kv_width), F32),
+    ]
+    held_bytes = 65536 + sum(a * b * jnp.dtype(kind).itemsize for (a, b), kind in results)
+    held = pl.pallas_call(
         functools.partial(step_kernel, n, dp),
-        out_shape=(dx_type, dq_type, jax.ShapeDtypeStruct(fin_shape, BF16)),
-        in_specs=[hbm] * 5 + [here] * 2 + [hbm] * 4,
-        out_specs=[hbm] * 3,
+        out_shape=[pltpu.VMEM(shape, kind) for shape, kind in results],
+        in_specs=[hbm] * 11,
+        out_specs=[here] * 4,
         scratch_shapes=scratch,
         compiler_params=pltpu.CompilerParams(
-            collective_id=0, has_side_effects=True, vmem_limit_bytes=56 * 1024 * 1024
+            collective_id=0, has_side_effects=True, vmem_limit_bytes=VMEM_BYTES - held_bytes
         ),
     )(
         inputs[0], queries[0], keys[0], values[0], out_grad[0],
@@ -634,14 +658,12 @@
     )
     dx, dq, kw, vw = pl.pallas_call(
         write_kernel,
-        out_shape=(dx_type, dq_type, kw_type, kw_type),
-        in_specs=[hbm] * 3,
+        out_shape=[jax.ShapeDtypeStruct(shape, kind) for shape, kind in results],
+        in_specs=[here] * 4,
         out_specs=[hbm] * 4,
-        scratch_shapes=[
-            vmem((rows, width), BF16), vmem((rows, q_width), BF16), vmem(fin_shape, BF16),
-            vmem((share, kv_width), F32), vmem((share, kv_width), F32), dma((3,)), dma((4,)),
-        ],
-    )(dx, dq, fin)
+        scratch_shapes=[dma((4,))],
+        compiler_params=pltpu.CompilerParams(vmem_limit_bytes=8 * 1024 * 1024),
+    )(*held)
     return dx[None], dq[None], kw, vw
 
 

time: 52 us -> 49.9 us (0.960); the launches traced: 51.3 us -> 49.8 us
  Pallas kernels: 50.7 us -> 49.1 us
    pallas_call x2, Pallas kernels: 50.7 us -> 49.1 us  [the longest x1 48.1 us: kernel_step(): pl.pallas_call(functools.partial(step_kernel, n, dp), out_shape=[pltpu.VM...]
where the time goes in v3:
time: 49.9 us; the launch traced here: 49.8 us
  Pallas kernels  49.1 us (98%)
  between operations  0.64 us (1%)
    pallas_call x1, Pallas kernels, kernel_step(): pl.pallas_call(functools.partial(step_kernel, n, dp), out_shape=[pltpu.VM...  48.1 us
    pallas_call x1, Pallas kernels, kernel_step(): pl.pallas_call(write_kernel, out_shape=[jax.ShapeDtypeStruct(shape, kind)...  1.09 us

profile of v3, /device:TPU:0, one launch (start us, length us, event | category | flops | bytes accessed | tf_op | source)
XLA Modules:
  0.0 49.8 jit_solution(16376835926710359950)
XLA Ops:
  0.6 48.1 %shard_map.138 = (bf16[128,2048]{1,0:T(8,128)(2,1)S(1)}, bf16[128,1024]{1,0:T(8,128)(2,1)S(1)}, f32[256,256]{1,0:T(8,128)S(1)}, f32[256,256]{1,0:T(8,128)S(1)}) custom-call(bf16[128,2048]{1,0:T(8,128)(2,1)} %bitcast.9, bf16[128,1024]{1,0:T(8,128)(2,1)} %bitcast.10, bf16[128,256]{1,0:T(8,128)(2,1)} %bitcast.12, bf16[128,256]{1,0:T(8,128)(2,1)} %bitcast.13, ...), custom_call_target="tpu_custom_call" | custom-call | tf_op jit(solution)/shard_map/pallas_call | solution.py:645
  48.7 1.1 %shard_map.139 = (bf16[128,2048]{1,0:T(8,128)(2,1)}, bf16[128,1024]{1,0:T(8,128)(2,1)}, f32[256,256]{1,0:T(8,128)}, f32[256,256]{1,0:T(8,128)}) custom-call(bf16[128,2048]{1,0:T(8,128)(2,1)S(1)} %get-tuple-element.12.refs_0_, bf16[128,1024]{1,0:T(8,128)(2,1)S(1)} %get-tuple-element.13.refs_1_, f32[256,256]{1,0:T(8,128)S(1)} %get-tuple-element.14.refs_2_, ...), custom_call_target="tpu_custom_call" | custom-call | tf_op jit(solution)/shard_map/pallas_call | solution.py:659

commit v4 on v3

--- a/solution.py
+++ b/solution.py
@@ -284,10 +284,10 @@
     x_hbm, q_hbm, k_hbm, v_hbm, do_hbm, qg_hbm, kg_hbm, km_hbm, vm_hbm, cos_hbm, sin_hbm,
     dx_buf, dq_buf, kw_buf, vw_buf,
     qg_ref, kg_ref, q_buf, do_buf, cos_buf, sin_buf, k_all, v_all, x_all, wk_all, wv_all,
-    q_st, do_st, k_st, v_st, dq_acc, part, got, far, g_all, x_t, wg_part, wg_got,
+    q_st, do_st, k_st, v_st, dq_acc, part, got, g_all, x_t, wg_part, wg_got,
     fin_all,
     local_sem, kv_send, kv_recv, x_send, x_recv, w_send, w_recv, w_fsend,
-    kv_fsend, far_send, far_recv, p_send, p_recv, g_send, g_recv, g_fsend, r_send, r_recv, f_send, f_recv,
+    p_send, p_recv, g_send, g_recv, g_fsend, r_send, r_recv, f_send, f_recv,
 ):
     me = lax.axis_index("sp")
     md = lax.axis_index("dp")
@@ -349,32 +349,20 @@
 
     sends = []
 
-    def only_if(condition, act):
-        if condition is None:
-            act()
-        else:
-            pl.when(condition)(act)
-
-    def send(*args, condition=None):
+    def send(*args):
         copy = remote(*args)
-        only_if(condition, copy.start)
-        sends.append((condition, copy))
+        copy.start()
+        sends.append(copy)
 
     def arrived(dst, recv):
         remote(dst, dst, recv, recv, {"sp": me}).wait_recv()
 
-    line = n == 4
-    near_right = {1: me != n - 1, n - 1: me != 0} if line else {}
-    near_left = {1: me != 0, n - 1: me != n - 1} if line else {}
-    inner = (me != 0) & (me != n - 1)
-    outer = (me == 0) | (me == n - 1)
-    inward = jnp.where(me == 0, 1, n - 2)
     order = sorted(range(1, n), key=lambda o: -min(o, n - o))
     for c in range(head_pairs):
         for kind, (src, dst) in enumerate([(k_hbm, k_all), (v_hbm, v_all)]):
             for o in order:
                 send(src.at[:, pair(c)], dst.at[c, me], kv_send.at[kind, c, o],
-                     kv_recv.at[kind, c, me], {"sp": sp_peer(o)}, condition=near_right.get(o))
+                     kv_recv.at[kind, c, me], {"sp": sp_peer(o)})
     weights = [(km_hbm, wk_all), (vm_hbm, wv_all)]
     for kind, (src, dst) in enumerate(weights):
         for o in range(2, dp, 2):
@@ -436,59 +424,28 @@
             dq_acc[:, head * HEAD_CHANNELS:head * HEAD_CHANNELS + LANES] = both.T
         return key_part, value_part
 
-    def add_far(c):
-        if not line:
-            return
-        across = sp_peer(2)
-        copy = remote(part.at[c, across], got.at[c, me], p_send.at[c, 2], p_recv.at[c, me],
-                      {"sp": across})
-
-        @pl.when(inner)
-        def _():
-            arrived(far.at[c], far_recv.at[c])
-            part[c, across] = (part[c, across].astype(F32) + far[c].astype(F32)).astype(BF16)
-            copy.start()
-
-        sends.append((inner, copy))
-
-    if line:
-        @pl.when(outer)
-        def _():
-            for c in range(head_pairs):
-                got[c, n - 1 - me] = jnp.zeros(got.shape[2:], BF16)
-
     for c in range(head_pairs):
         stack_keys(c, me)
     for c in range(head_pairs):
-        for o in order:
+        for o in range(1, n):
             src = sp_from(o)
-            for kind, ref in enumerate([k_all, v_all]):
-                arrived(ref.at[c, src], kv_recv.at[kind, c, src])
-                if line and o == 2:
-                    send(ref.at[c, src], ref.at[c, src], kv_fsend.at[kind, c],
-                         kv_recv.at[kind, c, src], {"sp": jnp.where(me == 1, 0, n - 1)},
-                         condition=inner)
+            arrived(k_all.at[c, src], kv_recv.at[0, c, src])
+            arrived(v_all.at[c, src], kv_recv.at[1, c, src])
             stack_keys(c, src)
-        if c:
-            add_far(c - 1)
         key_low, value_low = attend(2 * c)
         key_high, value_high = attend(2 * c + 1)
         both = jnp.concatenate([key_low, key_high, value_low, value_high], axis=1).astype(BF16)
         for j in range(n):
             part[c, j] = both[j * rows:(j + 1) * rows, :]
-        if line:
-            send(part.at[c, n - 1 - me], far.at[c], far_send.at[c], far_recv.at[c],
-                 {"sp": inward}, condition=outer)
         for o in order:
             send(part.at[c, sp_peer(o)], got.at[c, me], p_send.at[c, o], p_recv.at[c, me],
-                 {"sp": sp_peer(o)}, condition=outer if line and o == 2 else near_right.get(o))
-    add_far(head_pairs - 1)
+                 {"sp": sp_peer(o)})
 
     def own_grads(c):
         total = part[c, me].astype(F32)
         for o in range(1, n):
             src = sp_from(o)
-            only_if(near_left.get(o), functools.partial(arrived, got.at[c, src], p_recv.at[c, src]))
+            arrived(got.at[c, src], p_recv.at[c, src])
             total = total + got[c, src].astype(F32)
         g_all[c, md, :, :LANES] = norm_rotate_back(
             k_all[c, me].astype(F32), total[:, :LANES], k_gain, cos_own, sin_own
@@ -582,8 +539,8 @@
             at = pl.ds(pl.multiple_of(src * piece, piece), piece)
             kw_buf[at, pair(c)] = fin_all[c, src, :, :LANES].astype(F32)
             vw_buf[at, pair(c)] = fin_all[c, src, :, LANES:].astype(F32)
-    for condition, copy in sends:
-        only_if(condition, copy.wait_send)
+    for copy in sends:
+        copy.wait_send()
 
 
 def write_kernel(*refs):
@@ -623,14 +580,12 @@
         vmem((kv_heads, length, HEAD_CHANNELS), BF16), vmem((kv_heads, length, HEAD_CHANNELS), BF16),
         vmem((rows, q_width), F32),
         vmem((half, n, rows, wide), BF16), vmem((half, n, rows, wide), BF16),
-        vmem((half, rows, wide), BF16),
         vmem((half, dp, rows, wide), BF16), vmem((dp, share, rows), BF16),
         vmem((half, n, share // n, wide), BF16), vmem((half, n, share // n, wide), BF16),
         vmem((half, n, share // n, wide), BF16),
         dma((9 + 2 * half,)),
         dma((2, half, n)), dma((2, half, n)), dma((dp,)), dma((dp,)),
         dma((2, dp)), dma((2, dp)), dma((2, dp)),
-        dma((2, half)), dma((half,)), dma((half,)),
         dma((half, n)), dma((half, n)),
         dma((half, dp)), dma((half, dp)), dma((half, dp)),
         dma((half, n)), dma((half, n)), dma((half, n)), dma((half, n)),

time: 49.9 us -> 49.4 us (0.990)
  Pallas kernels: 49.1 us -> 48.6 us
    pallas_call x1, Pallas kernels: 48.1 us -> 47.5 us  [kernel_step(): pl.pallas_call(functools.partial(step_kernel, n, dp), out_shape=[pltpu.VM...]
where the time goes in v4:
time: 49.4 us; the launch traced here: 49.3 us
  Pallas kernels  48.6 us (98%)
  between operations  0.64 us (1%)
    pallas_call x1, Pallas kernels, kernel_step(): pl.pallas_call(functools.partial(step_kernel, n, dp), out_shape=[pltpu.VM...  47.5 us
    pallas_call x1, Pallas kernels, kernel_step(): pl.pallas_call(write_kernel, out_shape=[jax.ShapeDtypeStruct(shape, kind)...  1.09 us

profile of v4, /device:TPU:0, one launch (start us, length us, event | category | flops | bytes accessed | tf_op | source)
XLA Modules:
  0.0 49.3 jit_solution(6496725561633461637)
XLA Ops:
  0.6 47.5 %shard_map.138 = (bf16[128,2048]{1,0:T(8,128)(2,1)S(1)}, bf16[128,1024]{1,0:T(8,128)(2,1)S(1)}, f32[256,256]{1,0:T(8,128)S(1)}, f32[256,256]{1,0:T(8,128)S(1)}) custom-call(bf16[128,2048]{1,0:T(8,128)(2,1)} %bitcast.9, bf16[128,1024]{1,0:T(8,128)(2,1)} %bitcast.10, bf16[128,256]{1,0:T(8,128)(2,1)} %bitcast.12, bf16[128,256]{1,0:T(8,128)(2,1)} %bitcast.13, ...), custom_call_target="tpu_custom_call" | custom-call | tf_op jit(solution)/shard_map/pallas_call | solution.py:600
  48.2 1.1 %shard_map.139 = (bf16[128,2048]{1,0:T(8,128)(2,1)}, bf16[128,1024]{1,0:T(8,128)(2,1)}, f32[256,256]{1,0:T(8,128)}, f32[256,256]{1,0:T(8,128)}) custom-call(bf16[128,2048]{1,0:T(8,128)(2,1)S(1)} %get-tuple-element.12.refs_0_, bf16[128,1024]{1,0:T(8,128)(2,1)S(1)} %get-tuple-element.13.refs_1_, f32[256,256]{1,0:T(8,128)S(1)} %get-tuple-element.14.refs_2_, ...), custom_call_target="tpu_custom_call" | custom-call | tf_op jit(solution)/shard_map/pallas_call | solution.py:614
